TPU v7x, 32 devices: a whole 2x2x4 slice. The times are simulated.
32 devices in a mesh: sp: 8 (over z, y), tp: 4 (over x, core).
Axes of the slice: x: 2, y: 2, z: 4, core: 2. Of those that a mesh axis runs over, the one named last changes fastest.
Arguments:
- mixer_output_stream: bfloat16 [1024, 2048], P('sp', 'tp'), may hold values from -6 to 6
- layer_output_gradient: bfloat16 [1024, 2048], P('sp', 'tp'), may hold values from -2.5 to 2.5
- routes: int32 [1024, 2], P('sp'), may hold values from 0 to 7, all different within a row; in each aligned block of 128 rows (0 to 127, 128 to 255, ...) at most 48 rows name the same one
- expert_combine_weight: float32 [1024, 2], P('sp'), may hold values from 0.2 to 1
- expert_gate_weight: bfloat16 [8, 2048, 3584], P('sp', None, 'tp'), may hold values from -0.125 to 0.125
- expert_up_weight: bfloat16 [8, 2048, 3584], P('sp', None, 'tp'), may hold values from -0.125 to 0.125
- expert_down_weight: bfloat16 [8, 3584, 2048], P('sp', 'tp'), may hold values from -0.09375 to 0.09375
- head_mixer_input: bfloat16 [1024, 4096], P('sp', 'tp'), may hold values from -6 to 6
- head_step_size: float32 [1024, 64], P('sp', 'tp'), may hold values from 0.25 to 4
- head_decay_rate: float32 [64], P('tp'), may hold values from 0 to 1
- extra_log_decay: float32 [1024, 64], P('sp', 'tp'), may hold values from -3 to 0
- state_entering_span: float32 [64, 64, 128], P('tp'), may hold values from -48 to 48
- state_input_vectors: bfloat16 [1024, 1024], P('sp', 'tp'), may hold values from -1.75 to 1.75
- state_readout_vectors: bfloat16 [1024, 1024], P('sp', 'tp'), may hold values from -1.75 to 1.75
- gate_preactivation: bfloat16 [1024, 4096], P('sp', 'tp'), may hold values from -6 to 6
- group_norm_scale: float32 [4096], P('tp'), may hold values from 0.1 to 1.9
- mixer_output_weight: bfloat16 [4096, 2048], P('tp', 'sp'), may hold values from -0.09375 to 0.09375
Outputs:
- grad_gate: bfloat16 [8, 2048, 3584], P('sp', None, 'tp')
- grad_up: bfloat16 [8, 2048, 3584], P('sp', None, 'tp')
- grad_down: bfloat16 [8, 3584, 2048], P('sp', 'tp')
- grad_out_proj: float32 [4096, 2048], P('tp', 'sp')
- grad_input: bfloat16 [1024, 4096], P('sp', 'tp')
- grad_step: float32 [1024, 64], P('sp', 'tp')
- grad_state_in: bfloat16 [1024, 1024], P('sp', 'tp')
- grad_read_out: bfloat16 [1024, 1024], P('sp', 'tp')
- grad_gate_in: bfloat16 [1024, 4096], P('sp', 'tp')
Inputs may be any that keep to these rules, and one draw needn't show every extreme that they name: `routes`: the two experts of a token differ. In each aligned block of 128 rows no expert is named more than 48 times, and in every draw some expert is named exactly 48 times in some block.
All inputs are finite; a program needn't handle non-finite values.
Results may differ from a plain program's by a relative error of at most 0.02.
Values may be sent and summed in bfloat16 or wider, within the bound.
No kernel may reach another device: no remote copies, remote signals or barrier semaphores. Data moves between devices by JAX's collectives and lax.ppermute only.
A program may use at most 128 MiB of HBM per device.

v0:
```python
import functools
import jax
import jax.numpy as jnp
from jax import lax
from jax.experimental import pallas as pl
from jax.experimental.pallas import tpu as pltpu
from jax.sharding import PartitionSpec as P


HDIM = 64
STATE = 128
LANES = 2 * HDIM

norm_eps = 1e-05
exact_mode = lax.Precision.HIGHEST
F32, BF16 = jnp.float32, jnp.bfloat16
NN = (((1,), (0,)), ((), ()))
NT = (((1,), (1,)), ((), ()))
TN = (((0,), (0,)), ((), ()))


def mm(a, b, kind):
    return lax.dot_general(a, b, kind, preferred_element_type=F32)


def exact(a, b, kind):
    return lax.dot_general(a, b, kind, precision=exact_mode, preferred_element_type=F32)


def iota(shape, dim):
    return lax.broadcasted_iota(jnp.int32, shape, dim)


def lower_half(rows):
    return iota((rows, LANES), 1) < HDIM


def spread(cols, q):
    return jnp.where(
        lower_half(cols.shape[0]), cols[:, 2 * q : 2 * q + 1], cols[:, 2 * q + 1 : 2 * q + 2]
    )


def put_halves(total, value, q):
    low = lower_half(value.shape[0])
    at = iota(total.shape, 1)
    first = jnp.sum(jnp.where(low, value, 0.0), axis=1, keepdims=True)
    second = jnp.sum(jnp.where(low, 0.0, value), axis=1, keepdims=True)
    total = jnp.where(at == 2 * q, total + first, total)
    return jnp.where(at == 2 * q + 1, total + second, total)


def pair(q):
    return slice(q * LANES, (q + 1) * LANES)


def group_cols(ref, g):
    return ref[:, g * STATE : (g + 1) * STATE]


def log_decay(dt_ref, rate_ref, extra_ref):
    return extra_ref[...] - dt_ref[...] * rate_ref[...]


def running_sums(logs):
    length = logs.shape[0]
    up_to = (iota((length, length), 0) >= iota((length, length), 1)).astype(F32)
    return exact(up_to, logs, NN), exact(logs, up_to, (((0,), (1,)), ((), ())))


def log_rows(logs):
    whole = exact(logs, jnp.ones((logs.shape[0], LANES), F32), TN)
    return packed_logs(whole)


def packed_logs(whole):
    high = whole.astype(BF16).astype(F32)
    return jnp.where(lower_half(whole.shape[0]), high, whole - high).astype(BF16)


def unpacked_logs(rows):
    rows = rows.astype(F32)
    return jnp.broadcast_to(rows[:, :1] + rows[:, HDIM : HDIM + 1], rows.shape)


def state_kernel(x_ref, dt_ref, rate_ref, extra_ref, b_ref, out_ref):
    logs = log_decay(dt_ref, rate_ref, extra_ref)
    cum, _ = running_sums(logs)
    weight = dt_ref[...] * jnp.exp(cum[-1:] - cum)
    pairs = x_ref.shape[1] // LANES
    each = pairs // (b_ref.shape[1] // STATE)
    for q in range(pairs):
        scaled = (x_ref[:, pair(q)].astype(F32) * spread(weight, q)).astype(BF16)
        out_ref[pair(q), :] = mm(scaled, group_cols(b_ref, q // each), TN).astype(BF16)
    out_ref[x_ref.shape[1] :, :] = log_rows(logs)


def join_kernel(first, last, forward, use_ref, own_ref, got_ref, *refs):
    refs = list(refs)
    width = refs[-1].shape[0] if last else refs[-2].shape[0]
    heads = width // HDIM
    use = use_ref[0, 0]
    mine = unpacked_logs(own_ref[width:, :])
    other = unpacked_logs(got_ref[width:, :])
    if first:
        scale = jnp.full(mine.shape, use)
        gap = use * other
    else:
        before_ref, gap_ref = refs.pop(0), refs.pop(0)
        scale = use * jnp.exp(gap_ref[...])
        gap = gap_ref[...] + use * other
    if last and forward:
        entering_ref = refs.pop(0)
        keep = jnp.exp(gap)
    if not last:
        total_ref, prefix_ref, gap_out_ref = refs
        gap_out_ref[...] = gap
        from_got, from_own = jnp.exp(use * mine), jnp.exp((1.0 - use) * other)
        total_ref[width:, :] = packed_logs(mine + other)
    else:
        (prefix_ref,) = refs
    for h in range(heads):
        rows = slice(h * HDIM, (h + 1) * HDIM)
        got = got_ref[rows, :].astype(F32)
        value = scale[h : h + 1] * got
        if not first:
            value = value + before_ref[rows, :]
        if last and forward:
            value = value + keep[h : h + 1] * entering_ref[rows, :]
        prefix_ref[rows, :] = value.astype(prefix_ref.dtype)
        if not last:
            own = own_ref[rows, :].astype(F32)
            total_ref[rows, :] = (
                from_got[h : h + 1] * got + from_own[h : h + 1] * own
            ).astype(BF16)


def scan_kernel(
    x_ref, dt_ref, rate_ref, extra_ref, b_ref, c_ref, in_ref, z_ref, gain_ref, y_ref, normed_ref
):
    cum, cum_t = running_sums(log_decay(dt_ref, rate_ref, extra_ref))
    grown = jnp.exp(cum)
    length = cum.shape[0]
    causal = iota((length, length), 0) >= iota((length, length), 1)
    dt = dt_ref[...]
    groups = b_ref.shape[1] // STATE
    pairs = x_ref.shape[1] // LANES
    each = pairs // groups
    for g in range(groups):
        b_g, c_g = group_cols(b_ref, g), group_cols(c_ref, g)
        affinity = mm(c_g, b_g, NT)
        for q in range(g * each, (g + 1) * each):
            scaled = (x_ref[:, pair(q)].astype(F32) * spread(dt, q)).astype(BF16)
            parts = []
            for h in (2 * q, 2 * q + 1):
                gaps = cum[:, h : h + 1] - cum_t[h : h + 1, :]
                decays = jnp.where(causal, jnp.exp(jnp.where(causal, gaps, 0.0)), 0.0)
                parts.append(mm((affinity * decays).astype(BF16), scaled, NN))
            inside = jnp.where(lower_half(length), parts[0], parts[1])
            carried = mm(c_g, in_ref[pair(q), :].astype(BF16), NT)
            y_ref[:, pair(q)] = inside + carried * spread(grown, q)
        cols = slice(g * each * LANES, (g + 1) * each * LANES)
        z = z_ref[:, cols].astype(F32)
        gated = y_ref[:, cols] * (z * jax.nn.sigmoid(z))
        factor = lax.rsqrt(jnp.mean(gated * gated, axis=1, keepdims=True) + norm_eps)
        normed_ref[:, cols] = (gated * factor * gain_ref[:, cols]).astype(BF16)


def norm_back_kernel(
    blocks, dt_ref, rate_ref, extra_ref, c_ref, y_ref, z_ref, gain_ref, mix_ref, *refs
):
    w_refs, (dy_ref, dz_ref, reach_ref) = refs[:blocks], refs[blocks:]
    logs = log_decay(dt_ref, rate_ref, extra_ref)
    cum, _ = running_sums(logs)
    grown = jnp.exp(cum)
    groups = c_ref.shape[1] // STATE
    pairs = y_ref.shape[1] // LANES
    each = pairs // groups
    for g in range(groups):
        cols = slice(g * each * LANES, (g + 1) * each * LANES)
        up = mm(mix_ref[0], w_refs[0][cols, :], NT)
        for m in range(1, blocks):
            up = up + mm(mix_ref[m], w_refs[m][cols, :], NT)
        up = up * gain_ref[:, cols]
        z, y = z_ref[:, cols].astype(F32), y_ref[:, cols]
        sig = jax.nn.sigmoid(z)
        gated = y * (z * sig)
        factor = lax.rsqrt(jnp.mean(gated * gated, axis=1, keepdims=True) + norm_eps)
        shared = jnp.mean(up * gated, axis=1, keepdims=True) * factor * factor
        d_gated = factor * (up - gated * shared)
        dy_ref[:, cols] = (d_gated * (z * sig)).astype(BF16)
        dz_ref[:, cols] = (d_gated * y * sig * (1.0 + z * (1.0 - sig))).astype(BF16)
        c_g = group_cols(c_ref, g)
        for q in range(g * each, (g + 1) * each):
            weighted = (dy_ref[:, pair(q)].astype(F32) * spread(grown, q)).astype(BF16)
            reach_ref[pair(q), :] = mm(weighted, c_g, TN).astype(BF16)
    reach_ref[y_ref.shape[1] :, :] = log_rows(logs)


def inner_back_kernel(
    x_ref,
    dt_ref,
    rate_ref,
    extra_ref,
    b_ref,
    c_ref,
    in_ref,
    dy_ref,
    dx_ref,
    dc_ref,
    db_ref,
    at_ref,
    at_t_ref,
):
    cum, cum_t = running_sums(log_decay(dt_ref, rate_ref, extra_ref))
    grown = jnp.exp(cum)
    length = cum.shape[0]
    dt = dt_ref[...]
    later = iota((length, length), 1) >= iota((length, length), 0)
    low = lower_half(length)
    groups = b_ref.shape[1] // STATE
    pairs = x_ref.shape[1] // LANES
    each = pairs // groups
    at = jnp.zeros(cum.shape, F32)
    for g in range(groups):
        b_g, c_g = group_cols(b_ref, g), group_cols(c_ref, g)
        affinity = mm(b_g, c_g, NT)
        d_affinity = jnp.zeros((length, length), F32)
        dc = jnp.zeros((length, STATE), F32)
        for q in range(g * each, (g + 1) * each):
            scaled = (x_ref[:, pair(q)].astype(F32) * spread(dt, q)).astype(BF16)
            dy = dy_ref[:, pair(q)]
            parts = []
            for h in (2 * q, 2 * q + 1):
                gaps = cum_t[h : h + 1, :] - cum[:, h : h + 1]
                decays = jnp.where(later, jnp.exp(jnp.where(later, gaps, 0.0)), 0.0)
                half = jnp.where(low == (h % 2 == 0), scaled, jnp.zeros_like(scaled))
                back = mm(half, dy, NT)
                mixed = affinity * decays
                parts.append(mm(mixed.astype(BF16), dy, NN))
                moved = mixed * back
                d_affinity = d_affinity + decays * back
                lost = jnp.sum(moved, axis=1, keepdims=True)
                at = jnp.where(iota(at.shape, 1) == h, at - lost, at)
                at_t_ref[h : h + 1, :] = jnp.sum(moved, axis=0, keepdims=True)
            dx_ref[:, pair(q)] = jnp.where(low, parts[0], parts[1])
            held = in_ref[pair(q), :].astype(BF16)
            weighted = dy.astype(F32) * spread(grown, q)
            at = put_halves(at, weighted * mm(c_g, held, NT), q)
            dc = dc + mm(weighted.astype(BF16), held, NN)
        cols = slice(g * STATE, (g + 1) * STATE)
        d_affinity = d_affinity.astype(BF16)
        db_ref[:, cols] = mm(d_affinity, c_g, NN)
        dc_ref[:, cols] = (dc + mm(d_affinity, b_g, TN)).astype(BF16)
    at_ref[...] = at


def last_back_kernel(
    x_ref,
    dt_ref,
    rate_ref,
    extra_ref,
    b_ref,
    in_ref,
    later_ref,
    dx_ref,
    db_part_ref,
    at_ref,
    at_t_ref,
    d_input_ref,
    d_step_ref,
    db_ref,
):
    cum, _ = running_sums(log_decay(dt_ref, rate_ref, extra_ref))
    length, heads = cum.shape
    dt = dt_ref[...]
    to_end = jnp.exp(cum[-1:] - cum)
    groups = b_ref.shape[1] // STATE
    pairs = x_ref.shape[1] // LANES
    each = pairs // groups
    lost = jnp.zeros(cum.shape, F32)
    direct = jnp.zeros(cum.shape, F32)
    tail = jnp.zeros((1, heads), F32)
    for g in range(groups):
        b_g = group_cols(b_ref, g)
        db = db_part_ref[:, g * STATE : (g + 1) * STATE]
        for q in range(g * each, (g + 1) * each):
            grad = later_ref[pair(q), :]
            x = x_ref[:, pair(q)].astype(F32)
            scale = spread(dt, q)
            ending = spread(to_end, q)
            scaled = x * scale
            low_grad = grad.astype(BF16)
            dx_state = mm(b_g, low_grad, NT) * ending
            lost = put_halves(lost, scaled * dx_state, q)
            db = db + mm((scaled * ending).astype(BF16), low_grad, NN)
            dx = dx_ref[:, pair(q)] + dx_state
            d_input_ref[:, pair(q)] = (dx * scale).astype(BF16)
            direct = put_halves(direct, dx * x, q)
            kept = grad * in_ref[pair(q), :]
            for side in range(2):
                part = jnp.sum(kept[side * HDIM : (side + 1) * HDIM], axis=0, keepdims=True)
                part = jnp.sum(part, axis=1, keepdims=True)
                tail = jnp.where(iota(tail.shape, 1) == 2 * q + side, part, tail)
        db_ref[:, g * STATE : (g + 1) * STATE] = db.astype(BF16)
    from_here = (iota((length, length), 1) >= iota((length, length), 0)).astype(F32)
    d_log = exact(from_here, at_ref[...] - lost, NN) + exact(from_here, at_t_ref[...], NT)
    d_log = d_log + jnp.sum(lost, axis=0, keepdims=True) + jnp.exp(cum[-1:]) * tail
    d_step_ref[...] = (direct - d_log * rate_ref[...]).T


def call(kernel, outs, *args, scalars=0, name="kernel"):
    vmem, smem = pl.BlockSpec(memory_space=pltpu.VMEM), pl.BlockSpec(memory_space=pltpu.SMEM)
    return pl.pallas_call(
        kernel,
        out_shape=[jax.ShapeDtypeStruct(shape, kind) for shape, kind in outs],
        in_specs=[smem] * scalars + [vmem] * (len(args) - scalars),
        out_specs=[vmem] * len(outs),
        compiler_params=pltpu.CompilerParams(vmem_limit_bytes=(24 if name == "normback" else 12) << 20),
    )(*args)


def swapped(x, axis, mask):
    n = lax.axis_size(axis)
    return lax.ppermute(x, axis, [(i, i ^ mask) for i in range(n)])


def bits_of(n):
    return [1 << k for k in range(n.bit_length() - 1)]


def reorder(blocks, me, n):
    blocks = list(blocks)
    for bit in bits_of(n):
        is_set = (me & bit) != 0
        for m in range(n):
            if not m & bit:
                a, b = blocks[m], blocks[m | bit]
                blocks[m], blocks[m | bit] = jnp.where(is_set, b, a), jnp.where(is_set, a, b)
    return blocks


def gather_relative(x, axis):
    n = lax.axis_size(axis)
    blocks = {0: x}
    for bit in reversed(bits_of(n)):
        for m in sorted(blocks):
            blocks[m | bit] = swapped(blocks[m], axis, bit)
    return [blocks[m] for m in range(n)]


def exchange_relative(blocks, axis):
    swaps = [swapped(blocks[m], axis, m) for m in range(1, len(blocks))]
    return [blocks[0]] + swaps


def partner_kernel(width, spots, at_ref, x_ref, *refs):
    got_refs, out_ref = refs[:-1], refs[-1]
    for k in range(out_ref.shape[1] // width):
        start = pl.multiple_of(at_ref[0, k] * width, width)
        total = x_ref[:, pl.ds(start, width)].astype(F32)
        for got_ref, spot in zip(got_refs, spots):
            total = total + got_ref[:, spot[k] * width : (spot[k] + 1) * width].astype(F32)
        out_ref[:, k * width : (k + 1) * width] = total.astype(BF16)


def scatter_sum_columns(x, axis):
    n, me = lax.axis_size(axis), lax.axis_index(axis)
    width = x.shape[1] // n
    held, received = list(range(n)), []
    for bit in bits_of(n) + [0]:
        going = [m for m in held if m & bit] if bit else held
        spots = [[order.index(m) for m in going] for _, order in received]
        (sent,) = call(
            functools.partial(partner_kernel, width, spots),
            [((x.shape[0], width * len(going)), BF16)],
            jnp.stack([me ^ m for m in going]).astype(jnp.int32).reshape(1, -1),
            x,
            *[got for got, _ in received],
            scalars=1,
            name="sum",
        )
        if not bit:
            return sent
        held = [m for m in held if not m & bit]
        received.append((swapped(sent, axis, bit), held))


def exchange_steps(held, sent, axis, events):
    parts, sources = [held], [0]
    for bit in reversed(bits_of(held.shape[0])):
        if len(parts) > 1:
            rows = [part.reshape(-1, *part.shape[-3:])[:, bit : 2 * bit] for part in parts]
            sent = jnp.concatenate(rows, axis=0)
        got = swapped(sent, axis, bit)
        parts.append(after(got, events[len(parts) - 1]) if len(parts) <= len(events) else got)
        sources += [source | bit for source in sources]
    return parts, sources


def gather_steps(x, axis, moved):
    n = lax.axis_size(axis)
    offsets, blocks = [0], [x]
    for bit in reversed(bits_of(n)):
        for m, block in list(zip(offsets, blocks)):
            hop = bit
            if m in moved:
                hop = moved[m]
                block = blocks[offsets.index(m ^ hop ^ bit)]
            blocks.append(swapped(block, axis, hop))
            offsets.append(m | bit)
    return offsets, blocks


def after(x, *events):
    return lax.optimization_barrier((x, *events))[0]


def spread_states(own, widths, entering, forward, axis, name, seen=None):
    width, heads = widths
    n, me = lax.axis_size(axis), lax.axis_index(axis)
    bits = bits_of(n)
    state = []
    for step, bit in enumerate(bits):
        first, last = step == 0, bit == bits[-1]
        uses = ((me & bit) != 0) == forward
        use = jnp.where(uses, 1.0, 0.0).astype(F32).reshape(1, 1)
        args = [use, own, swapped(own, axis, bit)] + state
        outs = [((width, STATE), F32)]
        if last and forward:
            args.append(entering)
        if not last:
            outs = [(own.shape, BF16)] + outs + [((heads, LANES), F32)]
        made = call(functools.partial(join_kernel, first, last, forward), outs, *args, scalars=1, name=name + ("last" if last else "join"))
        if last:
            return made[0]
        own, state = made[0], list(made[1:])
        if seen is not None:
            seen.append(own)


def return_kernel(grad_ref, select_ref, *refs):
    blocks, out_ref = refs[:-1], refs[-1]
    total = grad_ref[...].astype(F32)
    for m, block in enumerate(blocks):
        total = total + mm(select_ref[m], block[...], TN)
    out_ref[...] = total.astype(BF16)


def proj_kernel(places, *refs):
    refs, out_ref = refs[:-1], refs[-1]
    normed, mixes = refs[: len(places)], refs[len(places) :]
    chunk = 2 * LANES
    rows = [mixes[0][0]]
    for mix in mixes[1:]:
        shape = mix.shape
        sources = shape[0] if len(shape) == 4 else 1
        rows += [mix[k, 0] if len(shape) == 4 else mix[0] for k in range(sources)]
    for c in range(0, out_ref.shape[0], chunk):
        total = jnp.zeros((chunk, out_ref.shape[1]), F32)
        for place, row in zip(places, rows):
            total = total + mm(normed[place][:, c : c + chunk], row, TN)
        out_ref[c : c + chunk, :] = total


def mix_kernel(place_ref, *refs):
    blocks, (mix_ref, sent_ref) = refs[:-2], refs[-2:]
    count, _, width = mix_ref.shape
    each = count // len(blocks)
    for m, block in enumerate(blocks):
        for part in range(each):
            at = place_ref[0, m * each + part]
            mix_ref[at] = block[:, part * width : (part + 1) * width]

            @pl.when(at >= count // 2)
            def _():
                sent_ref[at - count // 2] = block[:, part * width : (part + 1) * width]


def pack_kernel(experts, routes_ref, weight_ref, x_ref, grad_ref, packed_ref, select_ref):
    slots, tokens = select_ref.shape
    capacity = slots // experts
    width = x_ref.shape[1]
    numbers = iota((experts, tokens), 0)
    mask = jnp.zeros((experts, tokens), F32)
    weight = jnp.zeros((experts, tokens), F32)
    for k in range(routes_ref.shape[0]):
        chosen = routes_ref[k : k + 1, :] == numbers
        mask = jnp.where(chosen, 1.0, mask)
        weight = jnp.where(chosen, weight_ref[k : k + 1, :], weight)
    earlier = (iota((tokens, tokens), 0) < iota((tokens, tokens), 1)).astype(BF16)
    place = jnp.where(mask > 0.5, mm(mask.astype(BF16), earlier, NN), -1.0)
    row, number = iota((slots, experts), 0), iota((slots, experts), 1) * capacity
    owner = jnp.logical_and(row >= number, row < number + capacity).astype(F32)
    first = jnp.sum(owner * number.astype(F32), axis=1, keepdims=True)
    at_row = mm(owner.astype(BF16), place.astype(BF16), NN)
    at_slot = at_row + first == iota((slots, tokens), 0).astype(F32)
    at_slot = jnp.logical_and(at_slot, at_row > -0.5)
    of_row = exact(owner, weight, NN)
    slot_weight = jnp.sum(jnp.where(at_slot, of_row, 0.0), axis=1, keepdims=True)
    select = at_slot.astype(BF16)
    select_ref[...] = select
    packed_ref[:, :width] = mm(select, x_ref[...], NN).astype(BF16)
    packed_ref[:, width:] = (mm(select, grad_ref[...], NN) * slot_weight).astype(BF16)


def expert_hidden(routed_rows, routed_grads, w_gate, w_up, w_down):
    pre_gate = jnp.dot(routed_rows, w_gate, preferred_element_type=jnp.float32)
    pre_up = jnp.dot(routed_rows, w_up, preferred_element_type=jnp.float32)
    activated = jax.nn.silu(pre_gate)
    hidden = (activated * pre_up).astype(jnp.bfloat16)
    hidden_grad = lax.dot_general(
        routed_grads, w_down, (((1,), (1,)), ((), ())), preferred_element_type=jnp.float32
    )
    sigmoid_gate = jax.nn.sigmoid(pre_gate)
    gate_grad = (
        hidden_grad * pre_up * sigmoid_gate * (1.0 + pre_gate * (1.0 - sigmoid_gate))
    ).astype(jnp.bfloat16)
    up_grad = (hidden_grad * activated).astype(jnp.bfloat16)
    return (hidden, gate_grad, up_grad)


def expert_weight_grads(routed_rows, routed_grads, hidden, gate_grad, up_grad):
    contract = (((0,), (0,)), ((), ()))
    grad_g = lax.dot_general(routed_rows, gate_grad, contract, preferred_element_type=jnp.float32)
    grad_u = lax.dot_general(routed_rows, up_grad, contract, preferred_element_type=jnp.float32)
    grad_d = lax.dot_general(hidden, routed_grads, contract, preferred_element_type=jnp.float32)
    return (grad_g.astype(jnp.bfloat16), grad_u.astype(jnp.bfloat16), grad_d.astype(jnp.bfloat16))


def row_partial(gate_grad, up_grad, w_gate, w_up):
    contract = (((1,), (1,)), ((), ()))
    partial_sum = lax.dot_general(gate_grad, w_gate, contract, preferred_element_type=jnp.float32)
    partial_sum = partial_sum + lax.dot_general(
        up_grad, w_up, contract, preferred_element_type=jnp.float32
    )
    return partial_sum.astype(jnp.bfloat16)


def body(
    mixer_output_stream,
    layer_output_gradient,
    routes,
    expert_combine_weight,
    expert_gate_weight,
    expert_up_weight,
    expert_down_weight,
    head_mixer_input,
    head_step_size,
    head_decay_rate,
    extra_log_decay,
    state_entering_span,
    state_input_vectors,
    state_readout_vectors,
    gate_preactivation,
    group_norm_scale,
    mixer_output_weight,
):
    expert_count, me = lax.axis_size("sp"), lax.axis_index("sp")
    local_tokens, heads = head_step_size.shape
    width = head_mixer_input.shape[1]
    vectors = state_input_vectors.shape[1]
    capacity = 3 * local_tokens // expert_count
    w_gate = expert_gate_weight[0]
    w_up = expert_up_weight[0]
    w_down = expert_down_weight[0]
    rate = head_decay_rate[None, :]
    gain = group_norm_scale[None, :]
    entering = state_entering_span.reshape(width, STATE)

    slots = expert_count * capacity
    packed, select = call(
        functools.partial(pack_kernel, expert_count),
        [((slots, 2 * mixer_output_stream.shape[1]), BF16), ((slots, local_tokens), BF16)],
        routes.T ^ me,
        expert_combine_weight.T,
        mixer_output_stream,
        layer_output_gradient,
        name="pack",
    )
    packed, step_size = lax.optimization_barrier((packed, head_step_size))
    scan_args = (head_mixer_input, step_size, rate, extra_log_decay)
    rows = packed.reshape(expert_count, capacity, -1)
    received = exchange_relative([rows[m] for m in range(expert_count)], "sp")
    received = jnp.concatenate(received, axis=0)

    (own_state,) = call(
        state_kernel, [((width + heads, STATE), BF16)], *scan_args, state_input_vectors
    )
    part_width = mixer_output_stream.shape[1]
    gathered = gather_relative(received, "tp")
    gathered = reorder(gathered, lax.axis_index("tp"), lax.axis_size("tp"))
    routed_rows = jnp.concatenate([part[:, :part_width] for part in gathered], axis=1)
    routed_grads = jnp.concatenate([part[:, part_width:] for part in gathered], axis=1)
    hidden, gate_grad, up_grad = expert_hidden(routed_rows, routed_grads, w_gate, w_up, w_down)
    partial_rows = row_partial(gate_grad, up_grad, w_gate, w_up)
    summed = scatter_sum_columns(partial_rows, "tp")
    offsets, weights = gather_steps(after(mixer_output_weight, received), "sp", {})
    incoming = spread_states(
        own_state, (width, heads), entering, True, "sp", "f"
    )
    scan_out, normed = call(
        scan_kernel,
        [((local_tokens, width), F32), ((local_tokens, width), BF16)],
        *scan_args,
        state_input_vectors,
        state_readout_vectors,
        after(incoming, summed),
        gate_preactivation,
        gain,
    )
    summed = summed.reshape(expert_count, capacity, -1)
    returned = exchange_relative([summed[m] for m in range(expert_count)], "sp")
    (own_cols,) = call(
        return_kernel,
        [(layer_output_gradient.shape, BF16)],
        layer_output_gradient,
        select.reshape(expert_count, capacity, local_tokens),
        *returned,
        name="back",
    )
    grad_g, grad_u, grad_d = expert_weight_grads(
        routed_rows, routed_grads, hidden, gate_grad, up_grad
    )
    own_parts = gather_relative(own_cols, "tp")
    out_width = mixer_output_weight.shape[1]
    each = part_width // out_width
    numbers = jnp.arange(expert_count, dtype=jnp.int32)
    place = me ^ (((numbers // each) ^ lax.axis_index("tp")) * each + numbers % each)
    mix_parts, mix_sent = call(
        mix_kernel,
        [
            ((expert_count, local_tokens, out_width), BF16),
            ((expert_count // 2, local_tokens, out_width), BF16),
        ],
        place.reshape(1, -1),
        *own_parts,
        scalars=1,
        name="mix",
    )

    scan_grad, gate_grad_in, reached = call(
        functools.partial(norm_back_kernel, expert_count),
        [((local_tokens, width), BF16)] * 2 + [((width + heads, STATE), BF16)],
        *scan_args[1:],
        state_readout_vectors,
        scan_out,
        gate_preactivation,
        gain,
        mix_parts,
        *[weights[offsets.index(m)] for m in range(expert_count)],
        name="normback",
    )
    joined = []
    later = spread_states(reached, (width, heads), None, False, "sp", "b", joined)
    inner_x_grad, c_grad, inner_b_grad, at, at_t = call(
        inner_back_kernel,
        [
            ((local_tokens, width), F32),
            ((local_tokens, vectors), BF16),
            ((local_tokens, vectors), F32),
            ((local_tokens, heads), F32),
            ((heads, local_tokens), F32),
        ],
        *scan_args,
        state_input_vectors,
        state_readout_vectors,
        incoming,
        scan_grad,
        name="inner",
    )
    kept, all_normed = gather_steps(normed, "sp", {6: 2})
    all_mix, sources = exchange_steps(mix_parts, mix_sent, "sp", (grad_d, grad_u))
    input_grad, step_grad, b_grad = call(
        last_back_kernel,
        [
            ((local_tokens, width), BF16),
            ((heads, local_tokens), F32),
            ((local_tokens, vectors), BF16),
        ],
        *scan_args,
        state_input_vectors,
        incoming,
        later,
        inner_x_grad,
        inner_b_grad,
        at,
        at_t,
    )
    all_normed[-1] = after(all_normed[-1], step_grad)
    (proj_grad,) = call(
        functools.partial(proj_kernel, [kept.index(m) for m in sources]),
        [((width, out_width), F32)],
        *all_normed,
        *all_mix,
        name="proj",
    )
    return (
        grad_g[None],
        grad_u[None],
        grad_d[None],
        proj_grad,
        input_grad,
        step_grad.T,
        b_grad,
        c_grad,
        gate_grad_in,
    )


def solution(mesh):
    return jax.shard_map(
        body,
        mesh=mesh,
        in_specs=(
            P("sp", "tp"),
            P("sp", "tp"),
            P("sp", None),
            P("sp", None),
            P("sp", None, "tp"),
            P("sp", None, "tp"),
            P("sp", "tp", None),
            P("sp", "tp"),
            P("sp", "tp"),
            P("tp"),
            P("sp", "tp"),
            P("tp", None, None),
            P("sp", "tp"),
            P("sp", "tp"),
            P("sp", "tp"),
            P("tp"),
            P("tp", "sp"),
        ),
        out_specs=(
            P("sp", None, "tp"),
            P("sp", None, "tp"),
            P("sp", "tp", None),
            P("tp", "sp"),
            P("sp", "tp"),
            P("sp", "tp"),
            P("sp", "tp"),
            P("sp", "tp"),
            P("sp", "tp"),
        ),
        check_vma=False,
    )
```

profile of v0, /device:TPU:0, one launch (start us, length us, event | category | flops | bytes accessed | tf_op | source)
XLA Modules:
  0.0 241.7 jit_solution(6398165024508376695)
XLA Ops:
  5.2 3.1 %collective-permute-start = (bf16[48,1024]{1,0:T(8,128)(2,1)S(1)}, bf16[48,1024]{1,0:T(8,128)(2,1)S(1)}, u32[]{:S(2)}, u32[]{:S(2)}) collective-permute-start(bf16[48,1024]{1,0:T(8,128)(2,1)S(1)} %get-tuple-element.101), channel_id=1, source_target_pairs={{0,4},{4,0},{8,12},{12,8},{16,20},{20,16},{24,28},{28,24},{1,5},{5... | collective-permute-start | bytes 294920 | tf_op jit(solution)/shard_map/ppermute | solution.py:325
  8.3 3.5 %collective-permute-start.6 = (bf16[48,1024]{1,0:T(8,128)(2,1)S(1)}, bf16[48,1024]{1,0:T(8,128)(2,1)S(1)}, u32[]{:S(2)}, u32[]{:S(2)}) collective-permute-start(bf16[48,1024]{1,0:T(8,128)(2,1)S(1)} %get-tuple-element.95), channel_id=1, source_target_pairs={{0,28},{4,24},{8,20},{12,16},{16,12},{20,8},{24,4},{28,0},{1,29},{... | collective-permute-start | bytes 294920 | tf_op jit(solution)/shard_map/ppermute | solution.py:325
  13.8 2.1 collective-permute-start.3
  17.2 4.9 %collective-permute-done.1 = bf16[48,1024]{1,0:T(8,128)(2,1)S(1)} collective-permute-done((bf16[48,1024]{1,0:T(8,128)(2,1)S(1)}, bf16[48,1024]{1,0:T(8,128)(2,1)S(1)}, u32[]{:S(2)}, u32[]{:S(2)}) %collective-permute-start.1) | collective-permute-done | bytes 98336 | tf_op jit(solution)/shard_map/ppermute | solution.py:325
  22.1 3.4 %collective-permute-start.2 = (bf16[48,1024]{1,0:T(8,128)(2,1)S(1)}, bf16[48,1024]{1,0:T(8,128)(2,1)S(1)}, u32[]{:S(2)}, u32[]{:S(2)}) collective-permute-start(bf16[48,1024]{1,0:T(8,128)(2,1)S(1)} %get-tuple-element.99), channel_id=1, source_target_pairs={{0,12},{4,8},{8,4},{12,0},{16,28},{20,24},{24,20},{28,16},{1,13},{... | collective-permute-start | bytes 294920 | tf_op jit(solution)/shard_map/ppermute | solution.py:325
  25.5 5.4 %collective-permute-done.2 = bf16[48,1024]{1,0:T(8,128)(2,1)S(1)} collective-permute-done((bf16[48,1024]{1,0:T(8,128)(2,1)S(1)}, bf16[48,1024]{1,0:T(8,128)(2,1)S(1)}, u32[]{:S(2)}, u32[]{:S(2)}) %collective-permute-start.2) | collective-permute-done | bytes 98336 | tf_op jit(solution)/shard_map/ppermute | solution.py:325
  32.6 17.6 %collective-permute-done.7 = bf16[384,1024]{1,0:T(8,128)(2,1)S(1)} collective-permute-done((bf16[384,1024]{1,0:T(8,128)(2,1)S(1)}, bf16[384,1024]{1,0:T(8,128)(2,1)S(1)}, u32[]{:S(2)}, u32[]{:S(2)}) %collective-permute-start.7) | collective-permute-done | bytes 786464 | tf_op jit(solution)/shard_map/ppermute | solution.py:325
  50.2 2.3 collective-permute-done.8
  54.3 2.9 %copy-done.43 = bf16[1,2048,896]{2,1,0:T(8,128)(2,1)S(1)} copy-done((bf16[1,2048,896]{2,1,0:T(8,128)(2,1)S(1)}, bf16[1,2048,896]{2,1,0:T(8,128)(2,1)}, u32[]{:S(2)}) %copy-start.43) | copy-done | bytes 3670040
  61.7 3.0 %multiply_convert_fusion.1 = (bf16[384,896]{1,0:T(8,128)(2,1)S(1)}, bf16[384,896]{1,0:T(8,128)(2,1)S(1)}) fusion(f32[384,896]{1,0:T(8,128)S(1)} %fusion.2, f32[384,896]{1,0:T(8,128)S(1)} %fusion.6, bf16[1,896,2048]{2,1,0:T(8,128)(2,1)S(1)} %copy-done.42, bf16[384,512]{1,0:T(8,128)(2,1)S(1)} %get-tuple-element.114, ...), kind=kOutput, calls=%fused_computation.17 | convolution fusion | flops 1420050432 | bytes 9371648 | tf_op jit(solution)/shard_map/dot_general | solution.py:512
  74.9 5.2 %collective-permute-done.10.got_ref = bf16[1040,128]{1,0:T(8,128)(2,1)S(1)} collective-permute-done((bf16[1040,128]{1,0:T(8,128)(2,1)S(1)}, bf16[1040,128]{1,0:T(8,128)(2,1)S(1)}, u32[]{:S(2)}, u32[]{:S(2)}) %collective-permute-start.10) | collective-permute-done | bytes 266272 | tf_op jit(solution)/shard_map/ppermute | solution.py:325
  81.8 13.3 %collective-permute-done.35.refs_4_ = bf16[1024,256]{1,0:T(8,128)(2,1)} collective-permute-done((bf16[1024,256]{1,0:T(8,128)(2,1)}, bf16[1024,256]{1,0:T(8,128)(2,1)}, u32[]{:S(2)}, u32[]{:S(2)}) %collective-permute-start.35) | collective-permute-done | bytes 524320 | tf_op jit(solution)/shard_map/ppermute | solution.py:325
  95.0 11.7 %collective-permute-done.11.got_ref = bf16[1040,128]{1,0:T(8,128)(2,1)S(1)} collective-permute-done((bf16[1040,128]{1,0:T(8,128)(2,1)}, bf16[1040,128]{1,0:T(8,128)(2,1)S(1)}, u32[]{:S(2)}, u32[]{:S(2)}) %collective-permute-start.11) | collective-permute-done | bytes 266272 | tf_op jit(solution)/shard_map/ppermute | solution.py:325
  111.0 2.2 collective-permute-start.28
  120.3 9.8 %collective-permute-start.24 = (bf16[48,512]{1,0:T(8,128)(2,1)S(1)}, bf16[48,512]{1,0:T(8,128)(2,1)S(1)}, u32[]{:S(2)}, u32[]{:S(2)}) collective-permute-start(bf16[48,512]{1,0:T(8,128)(2,1)S(1)} %get-tuple-element.107), channel_id=1, source_target_pairs={{0,12},{4,8},{8,4},{12,0},{16,28},{20,24},{24,20},{28,16},{1,13},{... | collective-permute-start | bytes 147464 | tf_op jit(solution)/shard_map/ppermute | solution.py:325
  138.8 3.8 %collective-permute-done.30.refs_2_ = bf16[128,512]{1,0:T(8,128)(2,1)S(1)} collective-permute-done((bf16[128,512]{1,0:T(8,128)(2,1)S(1)}, bf16[128,512]{1,0:T(8,128)(2,1)S(1)}, u32[]{:S(2)}, u32[]{:S(2)}) %collective-permute-start.30) | collective-permute-done | bytes 131104 | tf_op jit(solution)/shard_map/ppermute | solution.py:325
  152.9 5.3 %collective-permute-done.36.refs_5_ = bf16[1024,256]{1,0:T(8,128)(2,1)} collective-permute-done((bf16[1024,256]{1,0:T(8,128)(2,1)}, bf16[1024,256]{1,0:T(8,128)(2,1)}, u32[]{:S(2)}, u32[]{:S(2)}) %collective-permute-start.36) | collective-permute-done | bytes 524320 | tf_op jit(solution)/shard_map/ppermute | solution.py:325
  158.2 11.2 %collective-permute-done.34.refs_3_ = bf16[1024,256]{1,0:T(8,128)(2,1)} collective-permute-done((bf16[1024,256]{1,0:T(8,128)(2,1)}, bf16[1024,256]{1,0:T(8,128)(2,1)}, u32[]{:S(2)}, u32[]{:S(2)}) %collective-permute-start.34) | collective-permute-done | bytes 524320 | tf_op jit(solution)/shard_map/ppermute | solution.py:325
  169.4 8.9 %collective-permute-done.38.refs_7_ = bf16[1024,256]{1,0:T(8,128)(2,1)} collective-permute-done((bf16[1024,256]{1,0:T(8,128)(2,1)}, bf16[1024,256]{1,0:T(8,128)(2,1)}, u32[]{:S(2)}, u32[]{:S(2)}) %collective-permute-start.38) | collective-permute-done | bytes 524320 | tf_op jit(solution)/shard_map/ppermute | solution.py:325
  178.4 5.8 %shard_map.243 = (bf16[128,1024]{1,0:T(8,128)(2,1)S(1)}, bf16[128,1024]{1,0:T(8,128)(2,1)}, bf16[1040,128]{1,0:T(8,128)(2,1)S(1)}) custom-call(f32[128,16]{1,0:T(8,128)S(1)} %copy.28.dt_ref, f32[1,16]{1,0:T(1,128)S(1)} %bitcast.57, f32[128,16]{1,0:T(8,128)S(1)} %copy.29.extra_ref, bf16[128,256]{1,0:T(8,128)(2,1)S(1)} %copy-done.3, ...), custom_call_target="tpu_custom_call" | custom-call | tf_op jit(solution)/shard_map/pallas_call | solution.py:314
  186.0 2.9 %collective-permute-start.42 = (bf16[4,128,256]{2,1,0:T(8,128)(2,1)}, bf16[4,128,256]{2,1,0:T(8,128)(2,1)S(1)}, u32[]{:S(2)}, u32[]{:S(2)}) collective-permute-start(bf16[4,128,256]{2,1,0:T(8,128)(2,1)} %copy-done.27), channel_id=1, source_target_pairs={{0,16},{4,20},{8,24},{12,28},{16,0},{20,4},{24,8},{28,12},{1,17},{... | collective-permute-start | bytes 786440 | tf_op jit(solution)/shard_map/ppermute | solution.py:325
  188.9 2.4 collective-permute-done.39.got_ref
  192.2 6.2 %convolution_convert_fusion = bf16[896,2048]{1,0:T(8,128)(2,1)} fusion(f32[384,896]{1,0:T(8,128)} %copy-done.50, bf16[384,512]{1,0:T(8,128)(2,1)} %copy-done.39, bf16[384,512]{1,0:T(8,128)(2,1)} %copy-done.38, bf16[384,512]{1,0:T(8,128)(2,1)} %copy-done.37, bf16[384,512]{1,0:T(8,128)(2,1)} %copy-done.36, f32[384,896]{1,0:T(8,128)} %copy-done.49), kind=kOutput, calls=%fused_computation.11 | convolution fusion | flops 1419476992 | bytes 7995392 | tf_op jit(solution)/shard_map/dot_general | solution.py:527
  199.9 3.9 %collective-permute-done.15.refs_1_ = bf16[128,1024]{1,0:T(8,128)(2,1)S(1)} collective-permute-done((bf16[128,1024]{1,0:T(8,128)(2,1)S(1)}, bf16[128,1024]{1,0:T(8,128)(2,1)S(1)}, u32[]{:S(2)}, u32[]{:S(2)}) %collective-permute-start.15) | collective-permute-done | bytes 262176 | tf_op jit(solution)/shard_map/ppermute | solution.py:325
  204.0 5.2 %collective-permute-done.42.refs_9_ = bf16[4,128,256]{2,1,0:T(8,128)(2,1)S(1)} collective-permute-done((bf16[4,128,256]{2,1,0:T(8,128)(2,1)}, bf16[4,128,256]{2,1,0:T(8,128)(2,1)S(1)}, u32[]{:S(2)}, u32[]{:S(2)}) %collective-permute-start.42) | collective-permute-done | bytes 262176 | tf_op jit(solution)/shard_map/ppermute | solution.py:325
  210.9 4.1 %convolution_convert_fusion.1 = bf16[2048,896]{1,0:T(8,128)(2,1)} fusion(bf16[384,896]{1,0:T(8,128)(2,1)S(1)} %copy-done.48, bf16[384,512]{1,0:T(8,128)(2,1)S(1)} %copy-done.35, bf16[384,512]{1,0:T(8,128)(2,1)S(1)} %copy-done.33, bf16[384,512]{1,0:T(8,128)(2,1)S(1)} %copy-done.31, bf16[384,512]{1,0:T(8,128)(2,1)S(1)} %copy-done.29), kind=kOutput, calls=%fused_computation.12 | convolution fusion | flops 1417412608 | bytes 5931008 | tf_op jit(solution)/shard_map/dot_general | solution.py:526
  215.4 4.2 %collective-permute-done.16.refs_2_ = bf16[128,1024]{1,0:T(8,128)(2,1)S(1)} collective-permute-done((bf16[128,1024]{1,0:T(8,128)(2,1)S(1)}, bf16[128,1024]{1,0:T(8,128)(2,1)S(1)}, u32[]{:S(2)}, u32[]{:S(2)}) %collective-permute-start.16) | collective-permute-done | bytes 262176 | tf_op jit(solution)/shard_map/ppermute | solution.py:325
  220.0 7.4 %collective-permute-done.43.refs_10_ = bf16[2,2,128,256]{3,2,1,0:T(8,128)(2,1)S(1)} collective-permute-done((bf16[2,2,128,256]{3,2,1,0:T(8,128)(2,1)S(1)}, bf16[2,2,128,256]{3,2,1,0:T(8,128)(2,1)S(1)}, u32[]{:S(2)}, u32[]{:S(2)}) %collective-permute-start.43) | collective-permute-done | bytes 262176 | tf_op jit(solution)/shard_map/ppermute | solution.py:325
  228.0 4.1 %convert_bitcast_fusion = bf16[1,2048,896]{2,1,0:T(8,128)(2,1)} fusion(bf16[384,896]{1,0:T(8,128)(2,1)S(1)} %copy-done.46, bf16[384,512]{1,0:T(8,128)(2,1)S(1)} %copy-done.35, bf16[384,512]{1,0:T(8,128)(2,1)S(1)} %copy-done.33, bf16[384,512]{1,0:T(8,128)(2,1)S(1)} %copy-done.31, bf16[384,512]{1,0:T(8,128)(2,1)S(1)} %copy-done.29), kind=kOutput, calls=%fused_computation.10 | convolution fusion | flops 1417412608 | bytes 5931008 | tf_op jit(solution)/shard_map/dot_general | solution.py:525
  232.1 4.5 %shard_map.247 = (f32[128,1024]{1,0:T(8,128)S(1)}, bf16[128,256]{1,0:T(8,128)(2,1)}, f32[128,256]{1,0:T(8,128)S(1)}, f32[128,16]{1,0:T(8,128)S(1)}, f32[16,128]{1,0:T(8,128)S(1)}) custom-call(bf16[128,1024]{1,0:T(8,128)(2,1)S(1)} %copy-done, f32[128,16]{1,0:T(8,128)S(1)} %copy.28.dt_ref, f32[1,16]{1,0:T(1,128)S(1)} %bitcast.58, ...), custom_call_target="tpu_custom_call" | custom-call | tf_op jit(solution)/shard_map/pallas_call | solution.py:314
  236.7 2.7 %shard_map.248 = (bf16[128,1024]{1,0:T(8,128)(2,1)}, f32[16,128]{1,0:T(8,128)}, bf16[128,256]{1,0:T(8,128)(2,1)}) custom-call(bf16[128,1024]{1,0:T(8,128)(2,1)S(1)} %copy-done, f32[128,16]{1,0:T(8,128)S(1)} %copy.28.dt_ref, f32[1,16]{1,0:T(1,128)S(1)} %bitcast.59, f32[128,16]{1,0:T(8,128)S(1)} %copy.29.extra_ref, bf16[128,256]{1,0:T(8,128)(2,1)S(1)} %copy-done.2, ...), custom_call_target="tpu_custom_call" | custom-call | tf_op jit(solution)/shard_map/pallas_call | solution.py:314
  239.5 2.3 shard_map.249
  (210 shorter events, 65.0 us)
Async XLA Ops:
  8.3 22.7 %collective-permute-start.6 = (bf16[48,1024]{1,0:T(8,128)(2,1)S(1)}, bf16[48,1024]{1,0:T(8,128)(2,1)S(1)}, u32[]{:S(2)}, u32[]{:S(2)}) collective-permute-start(bf16[48,1024]{1,0:T(8,128)(2,1)S(1)} %get-tuple-element.95), channel_id=1, source_target_pairs={{0,28},{4,24},{8,20},{12,16},{16,12},{20,8},{24,4},{28,0},{1,29},{... | collective-permute-start | bytes 294920 | tf_op jit(solution)/shard_map/ppermute | solution.py:325
  11.8 19.2 %collective-permute-start.5 = (bf16[48,1024]{1,0:T(8,128)(2,1)S(1)}, bf16[48,1024]{1,0:T(8,128)(2,1)S(1)}, u32[]{:S(2)}, u32[]{:S(2)}) collective-permute-start(bf16[48,1024]{1,0:T(8,128)(2,1)S(1)} %get-tuple-element.96), channel_id=1, source_target_pairs={{0,24},{4,28},{8,16},{12,20},{16,8},{20,12},{24,0},{28,4},{1,25},{... | collective-permute-start | bytes 294920 | tf_op jit(solution)/shard_map/ppermute | solution.py:325
  11.9 19.1 %collective-permute-start.4 = (bf16[48,1024]{1,0:T(8,128)(2,1)S(1)}, bf16[48,1024]{1,0:T(8,128)(2,1)S(1)}, u32[]{:S(2)}, u32[]{:S(2)}) collective-permute-start(bf16[48,1024]{1,0:T(8,128)(2,1)S(1)} %get-tuple-element.97), channel_id=1, source_target_pairs={{0,20},{4,16},{8,28},{12,24},{16,4},{20,0},{24,12},{28,8},{1,21},{... | collective-permute-start | bytes 294920 | tf_op jit(solution)/shard_map/ppermute | solution.py:325
  13.8 17.1 %collective-permute-start.3 = (bf16[48,1024]{1,0:T(8,128)(2,1)S(1)}, bf16[48,1024]{1,0:T(8,128)(2,1)S(1)}, u32[]{:S(2)}, u32[]{:S(2)}) collective-permute-start(bf16[48,1024]{1,0:T(8,128)(2,1)S(1)} %get-tuple-element.98), channel_id=1, source_target_pairs={{0,16},{4,20},{8,24},{12,28},{16,0},{20,4},{24,8},{28,12},{1,17},{... | collective-permute-start | bytes 294920 | tf_op jit(solution)/shard_map/ppermute | solution.py:325
  31.0 19.1 %collective-permute-start.7 = (bf16[384,1024]{1,0:T(8,128)(2,1)S(1)}, bf16[384,1024]{1,0:T(8,128)(2,1)S(1)}, u32[]{:S(2)}, u32[]{:S(2)}) collective-permute-start(bf16[384,1024]{1,0:T(8,128)(2,1)S(1)} %constant_dynamic-update-slice_fusion), channel_id=1, source_target_pairs={{0,2},{1,3},{2,0},{3,1},{4,6},{5,7},{6,4},{7,5},{8,10},{9,11},{10,... | collective-permute-start | bytes 2359304 | tf_op jit(solution)/shard_map/ppermute | solution.py:325
  32.6 17.7 %collective-permute-start.9 = (bf16[384,1024]{1,0:T(8,128)(2,1)S(1)}, bf16[384,1024]{1,0:T(8,128)(2,1)S(1)}, u32[]{:S(2)}, u32[]{:S(2)}) collective-permute-start(bf16[384,1024]{1,0:T(8,128)(2,1)S(1)} %constant_dynamic-update-slice_fusion), channel_id=1, source_target_pairs={{0,1},{1,0},{2,3},{3,2},{4,5},{5,4},{6,7},{7,6},{8,9},{9,8},{10,11... | collective-permute-start | bytes 2359304 | tf_op jit(solution)/shard_map/ppermute | solution.py:325
  70.2 24.9 %collective-permute-start.35 = (bf16[1024,256]{1,0:T(8,128)(2,1)}, bf16[1024,256]{1,0:T(8,128)(2,1)}, u32[]{:S(2)}, u32[]{:S(2)}) collective-permute-start(bf16[1024,256]{1,0:T(8,128)(2,1)} %refs_0_), channel_id=1, source_target_pairs={{0,16},{4,20},{8,24},{12,28},{16,0},{20,4},{24,8},{28,12},{1,17},{... | collective-permute-start | bytes 1572872 | tf_op jit(solution)/shard_map/ppermute | solution.py:325
  73.4 36.2 %collective-permute-start.14 = (bf16[384,512]{1,0:T(8,128)(2,1)}, bf16[384,512]{1,0:T(8,128)(2,1)}, u32[]{:S(2)}, u32[]{:S(2)}) collective-permute-start(bf16[384,512]{1,0:T(8,128)(2,1)} %shard_map.238), channel_id=1, source_target_pairs={{0,2},{1,3},{2,0},{3,1},{4,6},{5,7},{6,4},{7,5},{8,10},{9,11},{10,... | collective-permute-start | bytes 1179656 | tf_op jit(solution)/shard_map/ppermute | solution.py:325
  74.9 40.4 %collective-permute-start.33 = (bf16[1024,256]{1,0:T(8,128)(2,1)}, bf16[1024,256]{1,0:T(8,128)(2,1)}, u32[]{:S(2)}, u32[]{:S(2)}) collective-permute-start(bf16[1024,256]{1,0:T(8,128)(2,1)} %refs_0_), channel_id=1, source_target_pairs={{0,8},{4,12},{8,0},{12,4},{16,24},{20,28},{24,16},{28,20},{1,9},{5... | collective-permute-start | bytes 1572872 | tf_op jit(solution)/shard_map/ppermute | solution.py:325
  81.7 25.0 %collective-permute-start.11 = (bf16[1040,128]{1,0:T(8,128)(2,1)}, bf16[1040,128]{1,0:T(8,128)(2,1)S(1)}, u32[]{:S(2)}, u32[]{:S(2)}) collective-permute-start(bf16[1040,128]{1,0:T(8,128)(2,1)} %get-tuple-element.48.own_ref), channel_id=1, source_target_pairs={{0,8},{4,12},{8,0},{12,4},{16,24},{20,28},{24,16},{28,20},{1,9},{5... | collective-permute-start | bytes 798728 | tf_op jit(solution)/shard_map/ppermute | solution.py:325
  95.0 23.8 %collective-permute-start.37 = (bf16[1024,256]{1,0:T(8,128)(2,1)}, bf16[1024,256]{1,0:T(8,128)(2,1)}, u32[]{:S(2)}, u32[]{:S(2)}) collective-permute-start(bf16[1024,256]{1,0:T(8,128)(2,1)} %collective-permute-done.35.refs_4_), channel_id=1, source_target_pairs={{0,8},{4,12},{8,0},{12,4},{16,24},{20,28},{24,16},{28,20},{1,9},{5... | collective-permute-start | bytes 1572872 | tf_op jit(solution)/shard_map/ppermute | solution.py:325
  109.6 27.3 %collective-permute-start.12 = (bf16[1040,128]{1,0:T(8,128)(2,1)S(1)}, bf16[1040,128]{1,0:T(8,128)(2,1)S(1)}, u32[]{:S(2)}, u32[]{:S(2)}) collective-permute-start(bf16[1040,128]{1,0:T(8,128)(2,1)S(1)} %get-tuple-element.51.own_ref), channel_id=1, source_target_pairs={{0,16},{4,20},{8,24},{12,28},{16,0},{20,4},{24,8},{28,12},{1,17},{... | collective-permute-start | bytes 798728 | tf_op jit(solution)/shard_map/ppermute | solution.py:325
  113.2 16.9 %collective-permute-start.27 = (bf16[48,512]{1,0:T(8,128)(2,1)S(1)}, bf16[48,512]{1,0:T(8,128)(2,1)S(1)}, u32[]{:S(2)}, u32[]{:S(2)}) collective-permute-start(bf16[48,512]{1,0:T(8,128)(2,1)S(1)} %get-tuple-element.104), channel_id=1, source_target_pairs={{0,24},{4,28},{8,16},{12,20},{16,8},{20,12},{24,0},{28,4},{1,25},{... | collective-permute-start | bytes 147464 | tf_op jit(solution)/shard_map/ppermute | solution.py:325
  115.2 15.5 %collective-permute-start.26 = (bf16[48,512]{1,0:T(8,128)(2,1)S(1)}, bf16[48,512]{1,0:T(8,128)(2,1)S(1)}, u32[]{:S(2)}, u32[]{:S(2)}) collective-permute-start(bf16[48,512]{1,0:T(8,128)(2,1)S(1)} %get-tuple-element.105), channel_id=1, source_target_pairs={{0,20},{4,16},{8,28},{12,24},{16,4},{20,0},{24,12},{28,8},{1,21},{... | collective-permute-start | bytes 147464 | tf_op jit(solution)/shard_map/ppermute | solution.py:325
  118.9 12.9 %collective-permute-start.25 = (bf16[48,512]{1,0:T(8,128)(2,1)S(1)}, bf16[48,512]{1,0:T(8,128)(2,1)S(1)}, u32[]{:S(2)}, u32[]{:S(2)}) collective-permute-start(bf16[48,512]{1,0:T(8,128)(2,1)S(1)} %get-tuple-element.106), channel_id=1, source_target_pairs={{0,16},{4,20},{8,24},{12,28},{16,0},{20,4},{24,8},{28,12},{1,17},{... | collective-permute-start | bytes 147464 | tf_op jit(solution)/shard_map/ppermute | solution.py:325
  120.3 12.4 %collective-permute-start.24 = (bf16[48,512]{1,0:T(8,128)(2,1)S(1)}, bf16[48,512]{1,0:T(8,128)(2,1)S(1)}, u32[]{:S(2)}, u32[]{:S(2)}) collective-permute-start(bf16[48,512]{1,0:T(8,128)(2,1)S(1)} %get-tuple-element.107), channel_id=1, source_target_pairs={{0,12},{4,8},{8,4},{12,0},{16,28},{20,24},{24,20},{28,16},{1,13},{... | collective-permute-start | bytes 147464 | tf_op jit(solution)/shard_map/ppermute | solution.py:325
  131.8 21.1 %collective-permute-start.32 = (bf16[1024,256]{1,0:T(8,128)(2,1)}, bf16[1024,256]{1,0:T(8,128)(2,1)S(1)}, u32[]{:S(2)}, u32[]{:S(2)}) collective-permute-start(bf16[1024,256]{1,0:T(8,128)(2,1)} %refs_0_), channel_id=1, source_target_pairs={{0,4},{4,0},{8,12},{12,8},{16,20},{20,16},{24,28},{28,24},{1,5},{5... | collective-permute-start | bytes 1572872 | tf_op jit(solution)/shard_map/ppermute | solution.py:325
  132.7 25.5 %collective-permute-start.36 = (bf16[1024,256]{1,0:T(8,128)(2,1)}, bf16[1024,256]{1,0:T(8,128)(2,1)}, u32[]{:S(2)}, u32[]{:S(2)}) collective-permute-start(bf16[1024,256]{1,0:T(8,128)(2,1)} %collective-permute-done.35.refs_4_), channel_id=1, source_target_pairs={{0,4},{4,0},{8,12},{12,8},{16,20},{20,16},{24,28},{28,24},{1,5},{5... | collective-permute-start | bytes 1572872 | tf_op jit(solution)/shard_map/ppermute | solution.py:325
  134.2 35.3 %collective-permute-start.34 = (bf16[1024,256]{1,0:T(8,128)(2,1)}, bf16[1024,256]{1,0:T(8,128)(2,1)}, u32[]{:S(2)}, u32[]{:S(2)}) collective-permute-start(bf16[1024,256]{1,0:T(8,128)(2,1)} %collective-permute-done.33.refs_2_), channel_id=1, source_target_pairs={{0,4},{4,0},{8,12},{12,8},{16,20},{20,16},{24,28},{28,24},{1,5},{5... | collective-permute-start | bytes 1572872 | tf_op jit(solution)/shard_map/ppermute | solution.py:325
  135.6 42.8 %collective-permute-start.38 = (bf16[1024,256]{1,0:T(8,128)(2,1)}, bf16[1024,256]{1,0:T(8,128)(2,1)}, u32[]{:S(2)}, u32[]{:S(2)}) collective-permute-start(bf16[1024,256]{1,0:T(8,128)(2,1)} %collective-permute-done.37.refs_6_), channel_id=1, source_target_pairs={{0,4},{4,0},{8,12},{12,8},{16,20},{20,16},{24,28},{28,24},{1,5},{5... | collective-permute-start | bytes 1572872 | tf_op jit(solution)/shard_map/ppermute | solution.py:325
  186.0 17.7 %collective-permute-start.15 = (bf16[128,1024]{1,0:T(8,128)(2,1)S(1)}, bf16[128,1024]{1,0:T(8,128)(2,1)S(1)}, u32[]{:S(2)}, u32[]{:S(2)}) collective-permute-start(bf16[128,1024]{1,0:T(8,128)(2,1)S(1)} %get-tuple-element.55.refs_0_), channel_id=1, source_target_pairs={{0,16},{4,20},{8,24},{12,28},{16,0},{20,4},{24,8},{28,12},{1,17},{... | collective-permute-start | bytes 786440 | tf_op jit(solution)/shard_map/ppermute | solution.py:325
  186.0 23.2 %collective-permute-start.42 = (bf16[4,128,256]{2,1,0:T(8,128)(2,1)}, bf16[4,128,256]{2,1,0:T(8,128)(2,1)S(1)}, u32[]{:S(2)}, u32[]{:S(2)}) collective-permute-start(bf16[4,128,256]{2,1,0:T(8,128)(2,1)} %copy-done.27), channel_id=1, source_target_pairs={{0,16},{4,20},{8,24},{12,28},{16,0},{20,4},{24,8},{28,12},{1,17},{... | collective-permute-start | bytes 786440 | tf_op jit(solution)/shard_map/ppermute | solution.py:325
  191.6 18.9 %collective-permute-start.40 = (bf16[1040,128]{1,0:T(8,128)(2,1)S(1)}, bf16[1040,128]{1,0:T(8,128)(2,1)S(1)}, u32[]{:S(2)}, u32[]{:S(2)}) collective-permute-start(bf16[1040,128]{1,0:T(8,128)(2,1)S(1)} %get-tuple-element.61.own_ref), channel_id=1, source_target_pairs={{0,8},{4,12},{8,0},{12,4},{16,24},{20,28},{24,16},{28,20},{1,9},{5... | collective-permute-start | bytes 798728 | tf_op jit(solution)/shard_map/ppermute | solution.py:325
  198.4 21.2 %collective-permute-start.16 = (bf16[128,1024]{1,0:T(8,128)(2,1)S(1)}, bf16[128,1024]{1,0:T(8,128)(2,1)S(1)}, u32[]{:S(2)}, u32[]{:S(2)}) collective-permute-start(bf16[128,1024]{1,0:T(8,128)(2,1)S(1)} %get-tuple-element.55.refs_0_), channel_id=1, source_target_pairs={{0,8},{4,12},{8,0},{12,4},{16,24},{20,28},{24,16},{28,20},{1,9},{5... | collective-permute-start | bytes 786440 | tf_op jit(solution)/shard_map/ppermute | solution.py:325
  203.7 15.9 %collective-permute-start.19 = (bf16[128,1024]{1,0:T(8,128)(2,1)S(1)}, bf16[128,1024]{1,0:T(8,128)(2,1)S(1)}, u32[]{:S(2)}, u32[]{:S(2)}) collective-permute-start(bf16[128,1024]{1,0:T(8,128)(2,1)S(1)} %collective-permute-done.15.refs_1_), channel_id=1, source_target_pairs={{0,4},{4,0},{8,12},{12,8},{16,20},{20,16},{24,28},{28,24},{1,5},{5... | collective-permute-start | bytes 786440 | tf_op jit(solution)/shard_map/ppermute | solution.py:325
  209.3 18.1 %collective-permute-start.43 = (bf16[2,2,128,256]{3,2,1,0:T(8,128)(2,1)S(1)}, bf16[2,2,128,256]{3,2,1,0:T(8,128)(2,1)S(1)}, u32[]{:S(2)}, u32[]{:S(2)}) collective-permute-start(bf16[2,2,128,256]{3,2,1,0:T(8,128)(2,1)S(1)} %pad_maximum_fusion.4), channel_id=1, source_target_pairs={{0,8},{4,12},{8,0},{12,4},{16,24},{20,28},{24,16},{28,20},{1,9},{5... | collective-permute-start | bytes 786440 | tf_op jit(solution)/shard_map/ppermute | solution.py:325
  210.8 16.7 %collective-permute-start.41 = (bf16[1040,128]{1,0:T(8,128)(2,1)S(1)}, bf16[1040,128]{1,0:T(8,128)(2,1)S(1)}, u32[]{:S(2)}, u32[]{:S(2)}) collective-permute-start(bf16[1040,128]{1,0:T(8,128)(2,1)S(1)} %get-tuple-element.64.own_ref), channel_id=1, source_target_pairs={{0,16},{4,20},{8,24},{12,28},{16,0},{20,4},{24,8},{28,12},{1,17},{... | collective-permute-start | bytes 798728 | tf_op jit(solution)/shard_map/ppermute | solution.py:325
  215.0 24.4 %collective-permute-start.18 = (bf16[128,1024]{1,0:T(8,128)(2,1)S(1)}, bf16[128,1024]{1,0:T(8,128)(2,1)S(1)}, u32[]{:S(2)}, u32[]{:S(2)}) collective-permute-start(bf16[128,1024]{1,0:T(8,128)(2,1)S(1)} %get-tuple-element.55.refs_0_), channel_id=1, source_target_pairs={{0,4},{4,0},{8,12},{12,8},{16,20},{20,16},{24,28},{28,24},{1,5},{5... | collective-permute-start | bytes 786440 | tf_op jit(solution)/shard_map/ppermute | solution.py:325
  219.6 19.8 %collective-permute-start.17 = (bf16[128,1024]{1,0:T(8,128)(2,1)S(1)}, bf16[128,1024]{1,0:T(8,128)(2,1)S(1)}, u32[]{:S(2)}, u32[]{:S(2)}) collective-permute-start(bf16[128,1024]{1,0:T(8,128)(2,1)S(1)} %collective-permute-done.15.refs_1_), channel_id=1, source_target_pairs={{0,8},{4,12},{8,0},{12,4},{16,24},{20,28},{24,16},{28,20},{1,9},{5... | collective-permute-start | bytes 786440 | tf_op jit(solution)/shard_map/ppermute | solution.py:325
  219.6 19.8 %collective-permute-start.20 = (bf16[128,1024]{1,0:T(8,128)(2,1)S(1)}, bf16[128,1024]{1,0:T(8,128)(2,1)S(1)}, u32[]{:S(2)}, u32[]{:S(2)}) collective-permute-start(bf16[128,1024]{1,0:T(8,128)(2,1)S(1)} %collective-permute-done.16.refs_2_), channel_id=1, source_target_pairs={{0,4},{4,0},{8,12},{12,8},{16,20},{20,16},{24,28},{28,24},{1,5},{5... | collective-permute-start | bytes 786440 | tf_op jit(solution)/shard_map/ppermute | solution.py:325
  227.4 12.0 %collective-permute-start.21 = (bf16[128,1024]{1,0:T(8,128)(2,1)S(1)}, bf16[128,1024]{1,0:T(8,128)(2,1)S(1)}, u32[]{:S(2)}, u32[]{:S(2)}) collective-permute-start(bf16[128,1024]{1,0:T(8,128)(2,1)S(1)} %collective-permute-done.19.refs_5_), channel_id=1, source_target_pairs={{0,8},{4,12},{8,0},{12,4},{16,24},{20,28},{24,16},{28,20},{1,9},{5... | collective-permute-start | bytes 786440 | tf_op jit(solution)/shard_map/ppermute | solution.py:325
  227.5 11.9 %collective-permute-start.44 = (bf16[4,1,128,256]{3,2,1,0:T(8,128)(2,1)S(1)}, bf16[4,1,128,256]{3,2,1,0:T(8,128)(2,1)S(1)}, u32[]{:S(2)}, u32[]{:S(2)}) collective-permute-start(bf16[4,1,128,256]{3,2,1,0:T(8,128)(2,1)S(1)} %pad_maximum_fusion.5), channel_id=1, source_target_pairs={{0,4},{4,0},{8,12},{12,8},{16,20},{20,16},{24,28},{28,24},{1,5},{5... | collective-permute-start | bytes 786440 | tf_op jit(solution)/shard_map/ppermute | solution.py:325
  (64 other events, 527.7 us)
where the time goes:
time: 242 us
  waiting for transfers between devices  120 us (50%)
  starting transfers between devices  49.5 us (20%)
  Pallas kernels  26.3 us (11%)
  matrix products  24.7 us (10%)
  local copies, waits for them, and re-layouts  17.6 us (7%)
    ppermute x45, waiting for transfers between devices, swapped(): return lax.ppermute(x, axis, [(i, i ^ mask) for i in range(n)])  120 us
    ppermute x45, starting transfers between devices, swapped(): return lax.ppermute(x, axis, [(i, i ^ mask) for i in range(n)])  49.5 us
    pallas_call x18, Pallas kernels, call(): pl.pallas_call(kernel, out_shape=[jax.ShapeDtypeStruct(shape, kind) for s...  26.3 us
    unnamed x109, local copies, waits for them, and re-layouts  17.2 us
    dot_general x1, matrix products, expert_weight_grads(): lax.dot_general(hidden, routed_grads, contract, preferred_element_type=jn...  6.24 us
  transfers between devices with their start and end apart: 45, of which 23 were waited for; matrix products, arithmetic and copies ran while one was open for 6% of the time, Pallas kernels for 7%

commit v1 on v0

--- a/solution.py
+++ b/solution.py
@@ -354,6 +354,11 @@
     return [blocks[0]] + swaps
 
 
+def gather_columns(x, axis):
+    n = lax.axis_size(axis)
+    return jnp.concatenate(reorder(gather_relative(x, axis), lax.axis_index(axis), n), axis=1)
+
+
 def partner_kernel(width, spots, at_ref, x_ref, *refs):
     got_refs, out_ref = refs[:-1], refs[-1]
     for k in range(out_ref.shape[1] // width):
@@ -582,20 +587,19 @@
     scan_args = (head_mixer_input, step_size, rate, extra_log_decay)
     rows = packed.reshape(expert_count, capacity, -1)
     received = exchange_relative([rows[m] for m in range(expert_count)], "sp")
-    received = jnp.concatenate(received, axis=0)
 
     (own_state,) = call(
         state_kernel, [((width + heads, STATE), BF16)], *scan_args, state_input_vectors
     )
     part_width = mixer_output_stream.shape[1]
-    gathered = gather_relative(received, "tp")
-    gathered = reorder(gathered, lax.axis_index("tp"), lax.axis_size("tp"))
-    routed_rows = jnp.concatenate([part[:, :part_width] for part in gathered], axis=1)
-    routed_grads = jnp.concatenate([part[:, part_width:] for part in gathered], axis=1)
+    got_rows = jnp.concatenate([part[:, :part_width] for part in received], axis=0)
+    got_grads = jnp.concatenate([part[:, part_width:] for part in received], axis=0)
+    routed_rows = gather_columns(got_rows, "tp")
+    routed_grads = gather_columns(got_grads, "tp")
     hidden, gate_grad, up_grad = expert_hidden(routed_rows, routed_grads, w_gate, w_up, w_down)
     partial_rows = row_partial(gate_grad, up_grad, w_gate, w_up)
     summed = scatter_sum_columns(partial_rows, "tp")
-    offsets, weights = gather_steps(after(mixer_output_weight, received), "sp", {})
+    offsets, weights = gather_steps(after(mixer_output_weight, got_rows), "sp", {})
     incoming = spread_states(
         own_state, (width, heads), entering, True, "sp", "f"
     )

time: 242 us -> 238 us (0.983)
  waiting for transfers between devices: 120 us -> 105 us
  starting transfers between devices: 49.5 us -> 60.4 us
  local copies, waits for them, and re-layouts: 17.6 us -> 14.3 us
  matrix products: 24.7 us -> 27.3 us
    ppermute x45 -> x48, waiting for transfers between devices: 120 us -> 105 us  [swapped(): return lax.ppermute(x, axis, [(i, i ^ mask) for i in range(n)])]
    ppermute x45 -> x48, starting transfers between devices: 49.5 us -> 60.4 us  [swapped(): return lax.ppermute(x, axis, [(i, i ^ mask) for i in range(n)])]
    unnamed x109 -> x112, local copies, waits for them, and re-layouts: 17.2 us -> 14.1 us
    dot_general x1, matrix products: 1.8 us -> 4.4 us  [expert_hidden(): pre_gate = jnp.dot(routed_rows, w_gate, preferred_element_type=jnp.float32)]
  transfers between devices with their start and end apart: 45 -> 48, of which waited for: 23 -> 21; matrix products, arithmetic and copies ran while one was open for 6% -> 9% of each run, Pallas kernels for 7% -> 7%
where the time goes in v1:
time: 238 us; the launch traced here: 237 us
  waiting for transfers between devices  105 us (44%)
  starting transfers between devices  60.4 us (25%)
  matrix products  27.3 us (11%)
  Pallas kernels  26.3 us (11%)
  local copies, waits for them, and re-layouts  14.3 us (6%)
    ppermute x48, waiting for transfers between devices, swapped(): return lax.ppermute(x, axis, [(i, i ^ mask) for i in range(n)])  105 us
    ppermute x48, starting transfers between devices, swapped(): return lax.ppermute(x, axis, [(i, i ^ mask) for i in range(n)])  60.4 us
    pallas_call x18, Pallas kernels, call(): pl.pallas_call(kernel, out_shape=[jax.ShapeDtypeStruct(shape, kind) for s...  26.3 us
    unnamed x112, local copies, waits for them, and re-layouts  14.1 us
    dot_general x1, matrix products, expert_weight_grads(): lax.dot_general(hidden, routed_grads, contract, preferred_element_type=jn...  6.16 us
  transfers between devices with their start and end apart: 48, of which 21 were waited for; matrix products, arithmetic and copies ran while one was open for 9% of the time, Pallas kernels for 7%

profile of v1, /device:TPU:0, one launch (start us, length us, event | category | flops | bytes accessed | tf_op | source)
XLA Modules:
  0.0 237.2 jit_solution(9772802316588541178)
XLA Ops:
  4.6 6.1 %collective-permute-start.6 = (bf16[48,1024]{1,0:T(8,128)(2,1)S(1)}, bf16[48,1024]{1,0:T(8,128)(2,1)S(1)}, u32[]{:S(2)}, u32[]{:S(2)}) collective-permute-start(bf16[48,1024]{1,0:T(8,128)(2,1)S(1)} %get-tuple-element.93), channel_id=1, source_target_pairs={{0,28},{4,24},{8,20},{12,16},{16,12},{20,8},{24,4},{28,0},{1,29},{... | collective-permute-start | bytes 294920 | tf_op jit(solution)/shard_map/ppermute | solution.py:325
  15.3 3.0 %collective-permute-done = bf16[48,1024]{1,0:T(8,128)(2,1)S(1)} collective-permute-done((bf16[48,1024]{1,0:T(8,128)(2,1)S(1)}, bf16[48,1024]{1,0:T(8,128)(2,1)S(1)}, u32[]{:S(2)}, u32[]{:S(2)}) %collective-permute-start) | collective-permute-done | bytes 98336 | tf_op jit(solution)/shard_map/ppermute | solution.py:325
  18.3 2.3 collective-permute-start.1
  20.6 6.9 %collective-permute-done.1 = bf16[48,1024]{1,0:T(8,128)(2,1)S(1)} collective-permute-done((bf16[48,1024]{1,0:T(8,128)(2,1)S(1)}, bf16[48,1024]{1,0:T(8,128)(2,1)S(1)}, u32[]{:S(2)}, u32[]{:S(2)}) %collective-permute-start.1) | collective-permute-done | bytes 98336 | tf_op jit(solution)/shard_map/ppermute | solution.py:325
  28.1 4.9 %collective-permute-done.2 = bf16[48,1024]{1,0:T(8,128)(2,1)S(1)} collective-permute-done((bf16[48,1024]{1,0:T(8,128)(2,1)S(1)}, bf16[48,1024]{1,0:T(8,128)(2,1)S(1)}, u32[]{:S(2)}, u32[]{:S(2)}) %collective-permute-start.2) | collective-permute-done | bytes 98336 | tf_op jit(solution)/shard_map/ppermute | solution.py:325
  35.2 9.0 %collective-permute-done.7 = bf16[384,512]{1,0:T(8,128)(2,1)S(1)} collective-permute-done((bf16[384,512]{1,0:T(8,128)(2,1)S(1)}, bf16[384,512]{1,0:T(8,128)(2,1)S(1)}, u32[]{:S(2)}, u32[]{:S(2)}) %collective-permute-start.7) | collective-permute-done | bytes 393248 | tf_op jit(solution)/shard_map/ppermute | solution.py:325
  44.8 3.6 %collective-permute-done.10 = bf16[384,512]{1,0:T(8,128)(2,1)S(1)} collective-permute-done((bf16[384,512]{1,0:T(8,128)(2,1)S(1)}, bf16[384,512]{1,0:T(8,128)(2,1)S(1)}, u32[]{:S(2)}, u32[]{:S(2)}) %collective-permute-start.10) | collective-permute-done | bytes 393248 | tf_op jit(solution)/shard_map/ppermute | solution.py:325
  50.5 4.4 %fusion.2 = f32[384,896]{1,0:T(8,128)S(1)} fusion(bf16[1,2048,896]{2,1,0:T(8,128)(2,1)} %param.21, bf16[384,512]{1,0:T(8,128)(2,1)S(1)} %get-tuple-element.90, bf16[384,512]{1,0:T(8,128)(2,1)S(1)} %get-tuple-element.89, bf16[384,512]{1,0:T(8,128)(2,1)S(1)} %get-tuple-element.88, bf16[384,512]{1,0:T(8,128)(2,1)S(1)} %get-tuple-element.87), kind=kOutput, calls=%fused_computation.2 | convolution fusion | flops 1415577600 | bytes 6619136 | tf_op jit(solution)/shard_map/dot_general | solution.py:513
  57.5 3.0 %multiply_convert_fusion.1 = (bf16[384,896]{1,0:T(8,128)(2,1)S(1)}, bf16[384,896]{1,0:T(8,128)(2,1)S(1)}) fusion(f32[384,896]{1,0:T(8,128)S(1)} %fusion.2, f32[384,896]{1,0:T(8,128)S(1)} %fusion.6, bf16[1,896,2048]{2,1,0:T(8,128)(2,1)S(1)} %copy-done.43, bf16[384,512]{1,0:T(8,128)(2,1)S(1)} %get-tuple-element.86, ...), kind=kOutput, calls=%fused_computation.17 | convolution fusion | flops 1420050432 | bytes 9371648 | tf_op jit(solution)/shard_map/dot_general | solution.py:517
  71.7 2.6 %collective-permute-start.36 = (bf16[1024,256]{1,0:T(8,128)(2,1)}, bf16[1024,256]{1,0:T(8,128)(2,1)}, u32[]{:S(2)}, u32[]{:S(2)}) collective-permute-start(bf16[1024,256]{1,0:T(8,128)(2,1)} %refs_0_), channel_id=1, source_target_pairs={{0,8},{4,12},{8,0},{12,4},{16,24},{20,28},{24,16},{28,20},{1,9},{5... | collective-permute-start | bytes 1572872 | tf_op jit(solution)/shard_map/ppermute | solution.py:325
  78.1 2.6 %collective-permute-start.14 = (bf16[1040,128]{1,0:T(8,128)(2,1)}, bf16[1040,128]{1,0:T(8,128)(2,1)S(1)}, u32[]{:S(2)}, u32[]{:S(2)}) collective-permute-start(bf16[1040,128]{1,0:T(8,128)(2,1)} %get-tuple-element.48.own_ref), channel_id=1, source_target_pairs={{0,8},{4,12},{8,0},{12,4},{16,24},{20,28},{24,16},{28,20},{1,9},{5... | collective-permute-start | bytes 798728 | tf_op jit(solution)/shard_map/ppermute | solution.py:325
  80.7 12.0 %collective-permute-done.38.refs_4_ = bf16[1024,256]{1,0:T(8,128)(2,1)} collective-permute-done((bf16[1024,256]{1,0:T(8,128)(2,1)}, bf16[1024,256]{1,0:T(8,128)(2,1)}, u32[]{:S(2)}, u32[]{:S(2)}) %collective-permute-start.38) | collective-permute-done | bytes 524320 | tf_op jit(solution)/shard_map/ppermute | solution.py:325
  92.8 11.2 %collective-permute-done.14.got_ref = bf16[1040,128]{1,0:T(8,128)(2,1)S(1)} collective-permute-done((bf16[1040,128]{1,0:T(8,128)(2,1)}, bf16[1040,128]{1,0:T(8,128)(2,1)S(1)}, u32[]{:S(2)}, u32[]{:S(2)}) %collective-permute-start.14) | collective-permute-done | bytes 266272 | tf_op jit(solution)/shard_map/ppermute | solution.py:325
  114.0 4.0 %collective-permute-done.40.refs_6_ = bf16[1024,256]{1,0:T(8,128)(2,1)} collective-permute-done((bf16[1024,256]{1,0:T(8,128)(2,1)}, bf16[1024,256]{1,0:T(8,128)(2,1)}, u32[]{:S(2)}, u32[]{:S(2)}) %collective-permute-start.40) | collective-permute-done | bytes 524320 | tf_op jit(solution)/shard_map/ppermute | solution.py:325
  118.0 9.3 %collective-permute-start.27 = (bf16[48,512]{1,0:T(8,128)(2,1)S(1)}, bf16[48,512]{1,0:T(8,128)(2,1)S(1)}, u32[]{:S(2)}, u32[]{:S(2)}) collective-permute-start(bf16[48,512]{1,0:T(8,128)(2,1)S(1)} %get-tuple-element.104), channel_id=1, source_target_pairs={{0,12},{4,8},{8,4},{12,0},{16,28},{20,24},{24,20},{28,16},{1,13},{... | collective-permute-start | bytes 147464 | tf_op jit(solution)/shard_map/ppermute | solution.py:325
  135.3 4.3 %collective-permute-done.33.refs_2_ = bf16[128,512]{1,0:T(8,128)(2,1)S(1)} collective-permute-done((bf16[128,512]{1,0:T(8,128)(2,1)S(1)}, bf16[128,512]{1,0:T(8,128)(2,1)S(1)}, u32[]{:S(2)}, u32[]{:S(2)}) %collective-permute-start.33) | collective-permute-done | bytes 131104 | tf_op jit(solution)/shard_map/ppermute | solution.py:325
  149.9 4.9 %collective-permute-done.39.refs_5_ = bf16[1024,256]{1,0:T(8,128)(2,1)} collective-permute-done((bf16[1024,256]{1,0:T(8,128)(2,1)}, bf16[1024,256]{1,0:T(8,128)(2,1)}, u32[]{:S(2)}, u32[]{:S(2)}) %collective-permute-start.39) | collective-permute-done | bytes 524320 | tf_op jit(solution)/shard_map/ppermute | solution.py:325
  154.8 11.2 %collective-permute-done.37.refs_3_ = bf16[1024,256]{1,0:T(8,128)(2,1)} collective-permute-done((bf16[1024,256]{1,0:T(8,128)(2,1)}, bf16[1024,256]{1,0:T(8,128)(2,1)}, u32[]{:S(2)}, u32[]{:S(2)}) %collective-permute-start.37) | collective-permute-done | bytes 524320 | tf_op jit(solution)/shard_map/ppermute | solution.py:325
  166.1 7.9 %collective-permute-done.41.refs_7_ = bf16[1024,256]{1,0:T(8,128)(2,1)} collective-permute-done((bf16[1024,256]{1,0:T(8,128)(2,1)}, bf16[1024,256]{1,0:T(8,128)(2,1)}, u32[]{:S(2)}, u32[]{:S(2)}) %collective-permute-start.41) | collective-permute-done | bytes 524320 | tf_op jit(solution)/shard_map/ppermute | solution.py:325
  174.0 5.8 %shard_map.243 = (bf16[128,1024]{1,0:T(8,128)(2,1)S(1)}, bf16[128,1024]{1,0:T(8,128)(2,1)}, bf16[1040,128]{1,0:T(8,128)(2,1)S(1)}) custom-call(f32[128,16]{1,0:T(8,128)S(1)} %copy.28.dt_ref, f32[1,16]{1,0:T(1,128)S(1)} %bitcast.57, f32[128,16]{1,0:T(8,128)S(1)} %copy.29.extra_ref, bf16[128,256]{1,0:T(8,128)(2,1)S(1)} %copy-done.3, ...), custom_call_target="tpu_custom_call" | custom-call | tf_op jit(solution)/shard_map/pallas_call | solution.py:314
  181.5 2.9 %collective-permute-start.18 = (bf16[128,1024]{1,0:T(8,128)(2,1)S(1)}, bf16[128,1024]{1,0:T(8,128)(2,1)S(1)}, u32[]{:S(2)}, u32[]{:S(2)}) collective-permute-start(bf16[128,1024]{1,0:T(8,128)(2,1)S(1)} %get-tuple-element.55.refs_0_), channel_id=1, source_target_pairs={{0,16},{4,20},{8,24},{12,28},{16,0},{20,4},{24,8},{28,12},{1,17},{... | collective-permute-start | bytes 786440 | tf_op jit(solution)/shard_map/ppermute | solution.py:325
  184.4 2.5 %collective-permute-done.42.got_ref = bf16[1040,128]{1,0:T(8,128)(2,1)S(1)} collective-permute-done((bf16[1040,128]{1,0:T(8,128)(2,1)S(1)}, bf16[1040,128]{1,0:T(8,128)(2,1)S(1)}, u32[]{:S(2)}, u32[]{:S(2)}) %collective-permute-start.42) | collective-permute-done | bytes 266272 | tf_op jit(solution)/shard_map/ppermute | solution.py:325
  188.6 6.2 %convolution_convert_fusion = bf16[896,2048]{1,0:T(8,128)(2,1)} fusion(f32[384,896]{1,0:T(8,128)} %copy-done.51, bf16[384,512]{1,0:T(8,128)(2,1)} %copy-done.39, bf16[384,512]{1,0:T(8,128)(2,1)} %copy-done.38, bf16[384,512]{1,0:T(8,128)(2,1)} %copy-done.37, bf16[384,512]{1,0:T(8,128)(2,1)} %copy-done.36, f32[384,896]{1,0:T(8,128)} %copy-done.50), kind=kOutput, calls=%fused_computation.11 | convolution fusion | flops 1419476992 | bytes 7995392 | tf_op jit(solution)/shard_map/dot_general | solution.py:532
  195.5 4.9 %collective-permute-done.18.refs_1_ = bf16[128,1024]{1,0:T(8,128)(2,1)S(1)} collective-permute-done((bf16[128,1024]{1,0:T(8,128)(2,1)S(1)}, bf16[128,1024]{1,0:T(8,128)(2,1)S(1)}, u32[]{:S(2)}, u32[]{:S(2)}) %collective-permute-start.18) | collective-permute-done | bytes 262176 | tf_op jit(solution)/shard_map/ppermute | solution.py:325
  201.4 3.2 %collective-permute-done.45.refs_9_ = bf16[4,128,256]{2,1,0:T(8,128)(2,1)S(1)} collective-permute-done((bf16[4,128,256]{2,1,0:T(8,128)(2,1)}, bf16[4,128,256]{2,1,0:T(8,128)(2,1)S(1)}, u32[]{:S(2)}, u32[]{:S(2)}) %collective-permute-start.45) | collective-permute-done | bytes 262176 | tf_op jit(solution)/shard_map/ppermute | solution.py:325
  205.8 3.4 %collective-permute-start.44 = (bf16[1040,128]{1,0:T(8,128)(2,1)S(1)}, bf16[1040,128]{1,0:T(8,128)(2,1)S(1)}, u32[]{:S(2)}, u32[]{:S(2)}) collective-permute-start(bf16[1040,128]{1,0:T(8,128)(2,1)S(1)} %get-tuple-element.64.own_ref), channel_id=1, source_target_pairs={{0,16},{4,20},{8,24},{12,28},{16,0},{20,4},{24,8},{28,12},{1,17},{... | collective-permute-start | bytes 798728 | tf_op jit(solution)/shard_map/ppermute | solution.py:325
  209.2 4.1 %convolution_convert_fusion.1 = bf16[2048,896]{1,0:T(8,128)(2,1)} fusion(bf16[384,896]{1,0:T(8,128)(2,1)S(1)} %copy-done.49, bf16[384,512]{1,0:T(8,128)(2,1)S(1)} %copy-done.35, bf16[384,512]{1,0:T(8,128)(2,1)S(1)} %copy-done.33, bf16[384,512]{1,0:T(8,128)(2,1)S(1)} %copy-done.31, bf16[384,512]{1,0:T(8,128)(2,1)S(1)} %copy-done.29), kind=kOutput, calls=%fused_computation.12 | convolution fusion | flops 1417412608 | bytes 5931008 | tf_op jit(solution)/shard_map/dot_general | solution.py:531
  217.1 5.4 %collective-permute-done.46.refs_10_ = bf16[2,2,128,256]{3,2,1,0:T(8,128)(2,1)S(1)} collective-permute-done((bf16[2,2,128,256]{3,2,1,0:T(8,128)(2,1)S(1)}, bf16[2,2,128,256]{3,2,1,0:T(8,128)(2,1)S(1)}, u32[]{:S(2)}, u32[]{:S(2)}) %collective-permute-start.46) | collective-permute-done | bytes 262176 | tf_op jit(solution)/shard_map/ppermute | solution.py:325
  223.5 4.1 %convert_bitcast_fusion = bf16[1,2048,896]{2,1,0:T(8,128)(2,1)} fusion(bf16[384,896]{1,0:T(8,128)(2,1)S(1)} %copy-done.47, bf16[384,512]{1,0:T(8,128)(2,1)S(1)} %copy-done.35, bf16[384,512]{1,0:T(8,128)(2,1)S(1)} %copy-done.33, bf16[384,512]{1,0:T(8,128)(2,1)S(1)} %copy-done.31, bf16[384,512]{1,0:T(8,128)(2,1)S(1)} %copy-done.29), kind=kOutput, calls=%fused_computation.10 | convolution fusion | flops 1417412608 | bytes 5931008 | tf_op jit(solution)/shard_map/dot_general | solution.py:530
  227.6 4.5 %shard_map.247 = (f32[128,1024]{1,0:T(8,128)S(1)}, bf16[128,256]{1,0:T(8,128)(2,1)}, f32[128,256]{1,0:T(8,128)S(1)}, f32[128,16]{1,0:T(8,128)S(1)}, f32[16,128]{1,0:T(8,128)S(1)}) custom-call(bf16[128,1024]{1,0:T(8,128)(2,1)S(1)} %copy-done, f32[128,16]{1,0:T(8,128)S(1)} %copy.28.dt_ref, f32[1,16]{1,0:T(1,128)S(1)} %bitcast.58, ...), custom_call_target="tpu_custom_call" | custom-call | tf_op jit(solution)/shard_map/pallas_call | solution.py:314
  232.2 2.7 %shard_map.248 = (bf16[128,1024]{1,0:T(8,128)(2,1)}, f32[16,128]{1,0:T(8,128)}, bf16[128,256]{1,0:T(8,128)(2,1)}) custom-call(bf16[128,1024]{1,0:T(8,128)(2,1)S(1)} %copy-done, f32[128,16]{1,0:T(8,128)S(1)} %copy.28.dt_ref, f32[1,16]{1,0:T(1,128)S(1)} %bitcast.59, f32[128,16]{1,0:T(8,128)S(1)} %copy.29.extra_ref, bf16[128,256]{1,0:T(8,128)(2,1)S(1)} %copy-done.2, ...), custom_call_target="tpu_custom_call" | custom-call | tf_op jit(solution)/shard_map/pallas_call | solution.py:314
  234.9 2.3 shard_map.249
  (218 shorter events, 70.3 us)
Async XLA Ops:
  4.6 28.5 %collective-permute-start.6 = (bf16[48,1024]{1,0:T(8,128)(2,1)S(1)}, bf16[48,1024]{1,0:T(8,128)(2,1)S(1)}, u32[]{:S(2)}, u32[]{:S(2)}) collective-permute-start(bf16[48,1024]{1,0:T(8,128)(2,1)S(1)} %get-tuple-element.93), channel_id=1, source_target_pairs={{0,28},{4,24},{8,20},{12,16},{16,12},{20,8},{24,4},{28,0},{1,29},{... | collective-permute-start | bytes 294920 | tf_op jit(solution)/shard_map/ppermute | solution.py:325
  10.7 22.4 %collective-permute-start.5 = (bf16[48,1024]{1,0:T(8,128)(2,1)S(1)}, bf16[48,1024]{1,0:T(8,128)(2,1)S(1)}, u32[]{:S(2)}, u32[]{:S(2)}) collective-permute-start(bf16[48,1024]{1,0:T(8,128)(2,1)S(1)} %get-tuple-element.94), channel_id=1, source_target_pairs={{0,24},{4,28},{8,16},{12,20},{16,8},{20,12},{24,0},{28,4},{1,25},{... | collective-permute-start | bytes 294920 | tf_op jit(solution)/shard_map/ppermute | solution.py:325
  10.9 22.1 %collective-permute-start.4 = (bf16[48,1024]{1,0:T(8,128)(2,1)S(1)}, bf16[48,1024]{1,0:T(8,128)(2,1)S(1)}, u32[]{:S(2)}, u32[]{:S(2)}) collective-permute-start(bf16[48,1024]{1,0:T(8,128)(2,1)S(1)} %get-tuple-element.95), channel_id=1, source_target_pairs={{0,20},{4,16},{8,28},{12,24},{16,4},{20,0},{24,12},{28,8},{1,21},{... | collective-permute-start | bytes 294920 | tf_op jit(solution)/shard_map/ppermute | solution.py:325
  11.6 21.4 %collective-permute-start.3 = (bf16[48,1024]{1,0:T(8,128)(2,1)S(1)}, bf16[48,1024]{1,0:T(8,128)(2,1)S(1)}, u32[]{:S(2)}, u32[]{:S(2)}) collective-permute-start(bf16[48,1024]{1,0:T(8,128)(2,1)S(1)} %get-tuple-element.96), channel_id=1, source_target_pairs={{0,16},{4,20},{8,24},{12,28},{16,0},{20,4},{24,8},{28,12},{1,17},{... | collective-permute-start | bytes 294920 | tf_op jit(solution)/shard_map/ppermute | solution.py:325
  34.7 13.7 %collective-permute-start.10 = (bf16[384,512]{1,0:T(8,128)(2,1)S(1)}, bf16[384,512]{1,0:T(8,128)(2,1)S(1)}, u32[]{:S(2)}, u32[]{:S(2)}) collective-permute-start(bf16[384,512]{1,0:T(8,128)(2,1)S(1)} %get-tuple-element.108), channel_id=1, source_target_pairs={{0,2},{1,3},{2,0},{3,1},{4,6},{5,7},{6,4},{7,5},{8,10},{9,11},{10,... | collective-permute-start | bytes 1179656 | tf_op jit(solution)/shard_map/ppermute | solution.py:325
  35.2 13.2 %collective-permute-start.9 = (bf16[384,512]{1,0:T(8,128)(2,1)S(1)}, bf16[384,512]{1,0:T(8,128)(2,1)S(1)}, u32[]{:S(2)}, u32[]{:S(2)}) collective-permute-start(bf16[384,512]{1,0:T(8,128)(2,1)S(1)} %get-tuple-element.109), channel_id=1, source_target_pairs={{0,1},{1,0},{2,3},{3,2},{4,5},{5,4},{6,7},{7,6},{8,9},{9,8},{10,11... | collective-permute-start | bytes 1179656 | tf_op jit(solution)/shard_map/ppermute | solution.py:325
  44.3 12.5 %collective-permute-start.12 = (bf16[384,512]{1,0:T(8,128)(2,1)S(1)}, bf16[384,512]{1,0:T(8,128)(2,1)S(1)}, u32[]{:S(2)}, u32[]{:S(2)}) collective-permute-start(bf16[384,512]{1,0:T(8,128)(2,1)S(1)} %get-tuple-element.108), channel_id=1, source_target_pairs={{0,1},{1,0},{2,3},{3,2},{4,5},{5,4},{6,7},{7,6},{8,9},{9,8},{10,11... | collective-permute-start | bytes 1179656 | tf_op jit(solution)/shard_map/ppermute | solution.py:325
  66.4 26.4 %collective-permute-start.38 = (bf16[1024,256]{1,0:T(8,128)(2,1)}, bf16[1024,256]{1,0:T(8,128)(2,1)}, u32[]{:S(2)}, u32[]{:S(2)}) collective-permute-start(bf16[1024,256]{1,0:T(8,128)(2,1)} %refs_0_), channel_id=1, source_target_pairs={{0,16},{4,20},{8,24},{12,28},{16,0},{20,4},{24,8},{28,12},{1,17},{... | collective-permute-start | bytes 1572872 | tf_op jit(solution)/shard_map/ppermute | solution.py:325
  70.2 36.7 %collective-permute-start.17 = (bf16[384,512]{1,0:T(8,128)(2,1)}, bf16[384,512]{1,0:T(8,128)(2,1)}, u32[]{:S(2)}, u32[]{:S(2)}) collective-permute-start(bf16[384,512]{1,0:T(8,128)(2,1)} %shard_map.238), channel_id=1, source_target_pairs={{0,2},{1,3},{2,0},{3,1},{4,6},{5,7},{6,4},{7,5},{8,10},{9,11},{10,... | collective-permute-start | bytes 1179656 | tf_op jit(solution)/shard_map/ppermute | solution.py:325
  71.7 40.9 %collective-permute-start.36 = (bf16[1024,256]{1,0:T(8,128)(2,1)}, bf16[1024,256]{1,0:T(8,128)(2,1)}, u32[]{:S(2)}, u32[]{:S(2)}) collective-permute-start(bf16[1024,256]{1,0:T(8,128)(2,1)} %refs_0_), channel_id=1, source_target_pairs={{0,8},{4,12},{8,0},{12,4},{16,24},{20,28},{24,16},{28,20},{1,9},{5... | collective-permute-start | bytes 1572872 | tf_op jit(solution)/shard_map/ppermute | solution.py:325
  78.1 25.8 %collective-permute-start.14 = (bf16[1040,128]{1,0:T(8,128)(2,1)}, bf16[1040,128]{1,0:T(8,128)(2,1)S(1)}, u32[]{:S(2)}, u32[]{:S(2)}) collective-permute-start(bf16[1040,128]{1,0:T(8,128)(2,1)} %get-tuple-element.48.own_ref), channel_id=1, source_target_pairs={{0,8},{4,12},{8,0},{12,4},{16,24},{20,28},{24,16},{28,20},{1,9},{5... | collective-permute-start | bytes 798728 | tf_op jit(solution)/shard_map/ppermute | solution.py:325
  92.8 25.2 %collective-permute-start.40 = (bf16[1024,256]{1,0:T(8,128)(2,1)}, bf16[1024,256]{1,0:T(8,128)(2,1)}, u32[]{:S(2)}, u32[]{:S(2)}) collective-permute-start(bf16[1024,256]{1,0:T(8,128)(2,1)} %collective-permute-done.38.refs_4_), channel_id=1, source_target_pairs={{0,8},{4,12},{8,0},{12,4},{16,24},{20,28},{24,16},{28,20},{1,9},{5... | collective-permute-start | bytes 1572872 | tf_op jit(solution)/shard_map/ppermute | solution.py:325
  106.8 27.1 %collective-permute-start.15 = (bf16[1040,128]{1,0:T(8,128)(2,1)S(1)}, bf16[1040,128]{1,0:T(8,128)(2,1)S(1)}, u32[]{:S(2)}, u32[]{:S(2)}) collective-permute-start(bf16[1040,128]{1,0:T(8,128)(2,1)S(1)} %get-tuple-element.51.own_ref), channel_id=1, source_target_pairs={{0,16},{4,20},{8,24},{12,28},{16,0},{20,4},{24,8},{28,12},{1,17},{... | collective-permute-start | bytes 798728 | tf_op jit(solution)/shard_map/ppermute | solution.py:325
  110.5 16.8 %collective-permute-start.30 = (bf16[48,512]{1,0:T(8,128)(2,1)S(1)}, bf16[48,512]{1,0:T(8,128)(2,1)S(1)}, u32[]{:S(2)}, u32[]{:S(2)}) collective-permute-start(bf16[48,512]{1,0:T(8,128)(2,1)S(1)} %get-tuple-element.101), channel_id=1, source_target_pairs={{0,24},{4,28},{8,16},{12,20},{16,8},{20,12},{24,0},{28,4},{1,25},{... | collective-permute-start | bytes 147464 | tf_op jit(solution)/shard_map/ppermute | solution.py:325
  112.5 14.8 %collective-permute-start.29 = (bf16[48,512]{1,0:T(8,128)(2,1)S(1)}, bf16[48,512]{1,0:T(8,128)(2,1)S(1)}, u32[]{:S(2)}, u32[]{:S(2)}) collective-permute-start(bf16[48,512]{1,0:T(8,128)(2,1)S(1)} %get-tuple-element.102), channel_id=1, source_target_pairs={{0,20},{4,16},{8,28},{12,24},{16,4},{20,0},{24,12},{28,8},{1,21},{... | collective-permute-start | bytes 147464 | tf_op jit(solution)/shard_map/ppermute | solution.py:325
  118.0 11.5 %collective-permute-start.27 = (bf16[48,512]{1,0:T(8,128)(2,1)S(1)}, bf16[48,512]{1,0:T(8,128)(2,1)S(1)}, u32[]{:S(2)}, u32[]{:S(2)}) collective-permute-start(bf16[48,512]{1,0:T(8,128)(2,1)S(1)} %get-tuple-element.104), channel_id=1, source_target_pairs={{0,12},{4,8},{8,4},{12,0},{16,28},{20,24},{24,20},{28,16},{1,13},{... | collective-permute-start | bytes 147464 | tf_op jit(solution)/shard_map/ppermute | solution.py:325
  128.5 21.4 %collective-permute-start.35 = (bf16[1024,256]{1,0:T(8,128)(2,1)}, bf16[1024,256]{1,0:T(8,128)(2,1)S(1)}, u32[]{:S(2)}, u32[]{:S(2)}) collective-permute-start(bf16[1024,256]{1,0:T(8,128)(2,1)} %refs_0_), channel_id=1, source_target_pairs={{0,4},{4,0},{8,12},{12,8},{16,20},{20,16},{24,28},{28,24},{1,5},{5... | collective-permute-start | bytes 1572872 | tf_op jit(solution)/shard_map/ppermute | solution.py:325
  129.5 25.3 %collective-permute-start.39 = (bf16[1024,256]{1,0:T(8,128)(2,1)}, bf16[1024,256]{1,0:T(8,128)(2,1)}, u32[]{:S(2)}, u32[]{:S(2)}) collective-permute-start(bf16[1024,256]{1,0:T(8,128)(2,1)} %collective-permute-done.38.refs_4_), channel_id=1, source_target_pairs={{0,4},{4,0},{8,12},{12,8},{16,20},{20,16},{24,28},{28,24},{1,5},{5... | collective-permute-start | bytes 1572872 | tf_op jit(solution)/shard_map/ppermute | solution.py:325
  131.4 34.7 %collective-permute-start.37 = (bf16[1024,256]{1,0:T(8,128)(2,1)}, bf16[1024,256]{1,0:T(8,128)(2,1)}, u32[]{:S(2)}, u32[]{:S(2)}) collective-permute-start(bf16[1024,256]{1,0:T(8,128)(2,1)} %collective-permute-done.36.refs_2_), channel_id=1, source_target_pairs={{0,4},{4,0},{8,12},{12,8},{16,20},{20,16},{24,28},{28,24},{1,5},{5... | collective-permute-start | bytes 1572872 | tf_op jit(solution)/shard_map/ppermute | solution.py:325
  132.3 41.7 %collective-permute-start.41 = (bf16[1024,256]{1,0:T(8,128)(2,1)}, bf16[1024,256]{1,0:T(8,128)(2,1)}, u32[]{:S(2)}, u32[]{:S(2)}) collective-permute-start(bf16[1024,256]{1,0:T(8,128)(2,1)} %collective-permute-done.40.refs_6_), channel_id=1, source_target_pairs={{0,4},{4,0},{8,12},{12,8},{16,20},{20,16},{24,28},{28,24},{1,5},{5... | collective-permute-start | bytes 1572872 | tf_op jit(solution)/shard_map/ppermute | solution.py:325
  181.5 18.9 %collective-permute-start.18 = (bf16[128,1024]{1,0:T(8,128)(2,1)S(1)}, bf16[128,1024]{1,0:T(8,128)(2,1)S(1)}, u32[]{:S(2)}, u32[]{:S(2)}) collective-permute-start(bf16[128,1024]{1,0:T(8,128)(2,1)S(1)} %get-tuple-element.55.refs_0_), channel_id=1, source_target_pairs={{0,16},{4,20},{8,24},{12,28},{16,0},{20,4},{24,8},{28,12},{1,17},{... | collective-permute-start | bytes 786440 | tf_op jit(solution)/shard_map/ppermute | solution.py:325
  184.4 20.2 %collective-permute-start.45 = (bf16[4,128,256]{2,1,0:T(8,128)(2,1)}, bf16[4,128,256]{2,1,0:T(8,128)(2,1)S(1)}, u32[]{:S(2)}, u32[]{:S(2)}) collective-permute-start(bf16[4,128,256]{2,1,0:T(8,128)(2,1)} %copy-done.27), channel_id=1, source_target_pairs={{0,16},{4,20},{8,24},{12,28},{16,0},{20,4},{24,8},{28,12},{1,17},{... | collective-permute-start | bytes 786440 | tf_op jit(solution)/shard_map/ppermute | solution.py:325
  187.3 18.2 %collective-permute-start.43 = (bf16[1040,128]{1,0:T(8,128)(2,1)S(1)}, bf16[1040,128]{1,0:T(8,128)(2,1)S(1)}, u32[]{:S(2)}, u32[]{:S(2)}) collective-permute-start(bf16[1040,128]{1,0:T(8,128)(2,1)S(1)} %get-tuple-element.61.own_ref), channel_id=1, source_target_pairs={{0,8},{4,12},{8,0},{12,4},{16,24},{20,28},{24,16},{28,20},{1,9},{5... | collective-permute-start | bytes 798728 | tf_op jit(solution)/shard_map/ppermute | solution.py:325
  194.7 21.4 %collective-permute-start.19 = (bf16[128,1024]{1,0:T(8,128)(2,1)S(1)}, bf16[128,1024]{1,0:T(8,128)(2,1)S(1)}, u32[]{:S(2)}, u32[]{:S(2)}) collective-permute-start(bf16[128,1024]{1,0:T(8,128)(2,1)S(1)} %get-tuple-element.55.refs_0_), channel_id=1, source_target_pairs={{0,8},{4,12},{8,0},{12,4},{16,24},{20,28},{24,16},{28,20},{1,9},{5... | collective-permute-start | bytes 786440 | tf_op jit(solution)/shard_map/ppermute | solution.py:325
  200.4 15.7 %collective-permute-start.22 = (bf16[128,1024]{1,0:T(8,128)(2,1)S(1)}, bf16[128,1024]{1,0:T(8,128)(2,1)S(1)}, u32[]{:S(2)}, u32[]{:S(2)}) collective-permute-start(bf16[128,1024]{1,0:T(8,128)(2,1)S(1)} %collective-permute-done.18.refs_1_), channel_id=1, source_target_pairs={{0,4},{4,0},{8,12},{12,8},{16,20},{20,16},{24,28},{28,24},{1,5},{5... | collective-permute-start | bytes 786440 | tf_op jit(solution)/shard_map/ppermute | solution.py:325
  204.7 17.8 %collective-permute-start.46 = (bf16[2,2,128,256]{3,2,1,0:T(8,128)(2,1)S(1)}, bf16[2,2,128,256]{3,2,1,0:T(8,128)(2,1)S(1)}, u32[]{:S(2)}, u32[]{:S(2)}) collective-permute-start(bf16[2,2,128,256]{3,2,1,0:T(8,128)(2,1)S(1)} %pad_maximum_fusion.4), channel_id=1, source_target_pairs={{0,8},{4,12},{8,0},{12,4},{16,24},{20,28},{24,16},{28,20},{1,9},{5... | collective-permute-start | bytes 786440 | tf_op jit(solution)/shard_map/ppermute | solution.py:325
  205.8 16.7 %collective-permute-start.44 = (bf16[1040,128]{1,0:T(8,128)(2,1)S(1)}, bf16[1040,128]{1,0:T(8,128)(2,1)S(1)}, u32[]{:S(2)}, u32[]{:S(2)}) collective-permute-start(bf16[1040,128]{1,0:T(8,128)(2,1)S(1)} %get-tuple-element.64.own_ref), channel_id=1, source_target_pairs={{0,16},{4,20},{8,24},{12,28},{16,0},{20,4},{24,8},{28,12},{1,17},{... | collective-permute-start | bytes 798728 | tf_op jit(solution)/shard_map/ppermute | solution.py:325
  213.3 21.6 %collective-permute-start.21 = (bf16[128,1024]{1,0:T(8,128)(2,1)S(1)}, bf16[128,1024]{1,0:T(8,128)(2,1)S(1)}, u32[]{:S(2)}, u32[]{:S(2)}) collective-permute-start(bf16[128,1024]{1,0:T(8,128)(2,1)S(1)} %get-tuple-element.55.refs_0_), channel_id=1, source_target_pairs={{0,4},{4,0},{8,12},{12,8},{16,20},{20,16},{24,28},{28,24},{1,5},{5... | collective-permute-start | bytes 786440 | tf_op jit(solution)/shard_map/ppermute | solution.py:325
  216.1 18.8 %collective-permute-start.20 = (bf16[128,1024]{1,0:T(8,128)(2,1)S(1)}, bf16[128,1024]{1,0:T(8,128)(2,1)S(1)}, u32[]{:S(2)}, u32[]{:S(2)}) collective-permute-start(bf16[128,1024]{1,0:T(8,128)(2,1)S(1)} %collective-permute-done.18.refs_1_), channel_id=1, source_target_pairs={{0,8},{4,12},{8,0},{12,4},{16,24},{20,28},{24,16},{28,20},{1,9},{5... | collective-permute-start | bytes 786440 | tf_op jit(solution)/shard_map/ppermute | solution.py:325
  216.1 18.8 %collective-permute-start.23 = (bf16[128,1024]{1,0:T(8,128)(2,1)S(1)}, bf16[128,1024]{1,0:T(8,128)(2,1)S(1)}, u32[]{:S(2)}, u32[]{:S(2)}) collective-permute-start(bf16[128,1024]{1,0:T(8,128)(2,1)S(1)} %collective-permute-done.19.refs_2_), channel_id=1, source_target_pairs={{0,4},{4,0},{8,12},{12,8},{16,20},{20,16},{24,28},{28,24},{1,5},{5... | collective-permute-start | bytes 786440 | tf_op jit(solution)/shard_map/ppermute | solution.py:325
  222.4 12.5 %collective-permute-start.24 = (bf16[128,1024]{1,0:T(8,128)(2,1)S(1)}, bf16[128,1024]{1,0:T(8,128)(2,1)S(1)}, u32[]{:S(2)}, u32[]{:S(2)}) collective-permute-start(bf16[128,1024]{1,0:T(8,128)(2,1)S(1)} %collective-permute-done.22.refs_5_), channel_id=1, source_target_pairs={{0,8},{4,12},{8,0},{12,4},{16,24},{20,28},{24,16},{28,20},{1,9},{5... | collective-permute-start | bytes 786440 | tf_op jit(solution)/shard_map/ppermute | solution.py:325
  222.5 12.4 %collective-permute-start.47 = (bf16[4,1,128,256]{3,2,1,0:T(8,128)(2,1)S(1)}, bf16[4,1,128,256]{3,2,1,0:T(8,128)(2,1)S(1)}, u32[]{:S(2)}, u32[]{:S(2)}) collective-permute-start(bf16[4,1,128,256]{3,2,1,0:T(8,128)(2,1)S(1)} %pad_maximum_fusion.5), channel_id=1, source_target_pairs={{0,4},{4,0},{8,12},{12,8},{16,20},{20,16},{24,28},{28,24},{1,5},{5... | collective-permute-start | bytes 786440 | tf_op jit(solution)/shard_map/ppermute | solution.py:325
  (68 other events, 571.3 us)
